TPU v7x, 256 devices: a whole 4x4x8 slice. The times are simulated.
256 devices in a mesh: sp: 64 (over z, x, core), tp: 4 (over y).
Axes of the slice: x: 4, y: 4, z: 8, core: 2. Of those that a mesh axis runs over, the one named last changes fastest.
Arguments:
- tokens: bfloat16 [16384, 1024], P(('sp', 'tp')), may hold values from -6 to 6
- norm_gain: float32 [1024], replicated, may hold values from 0.1 to 1.9
- w_query: bfloat16 [1024, 1024], P('sp', 'tp'), may hold values from -0.1875 to 0.1875
- w_key: bfloat16 [1024, 1024], P('sp', 'tp'), may hold values from -0.1875 to 0.1875
- w_value: bfloat16 [1024, 1024], P('sp', 'tp'), may hold values from -0.1875 to 0.1875
- w_forget: bfloat16 [1024, 16], P('sp', 'tp'), may hold values from -0.375 to 0.375
- forget_offset: float32 [16], P('tp'), may hold values from 1 to 3.5
- w_out_t: bfloat16 [1024, 1024], P('sp', 'tp'), may hold values from -0.1875 to 0.1875
- out_gain: float32 [1024], replicated, may hold values from 0.1 to 1.9
Outputs:
- mixed: bfloat16 [16384, 1024], P(('sp', 'tp'))
All inputs are finite; a program needn't handle non-finite values.
Results may differ from a plain program's by a relative error of at most 0.015.
Values may be sent and summed in bfloat16 or wider, within the bound.
A program may use at most 192 MiB of HBM per device.

v0:
```python
import functools

import jax
import jax.numpy as jnp
from jax import lax
from jax.experimental import pallas as pl
from jax.experimental.pallas import tpu as pltpu
from jax.sharding import PartitionSpec as P

HEAD_DIM = 64
LANES = 128
NORM_EPS = 1e-06
MESH = pl.DeviceIdType.MESH
F32 = jnp.float32
BF16 = jnp.bfloat16
CONTRACT_LAST = (((1,), (1,)), ((), ()))


def rms_norm(floats, gain_row):
    scale_col = lax.rsqrt(jnp.mean(floats * floats, axis=-1, keepdims=True) + NORM_EPS)
    return (floats * scale_col * gain_row).astype(BF16)


def layer_kernel(
    n_sp, n_tp, heads,
    tokens_ref, gain_ref, wq_ref, wk_ref, wv_ref, wf_ref, offset_ref, wo_ref, out_gain_ref,
    out_ref,
    normed, w_all, wo_all, kv_all, forget_all, gates, q_heads, cum_query, run_max, run_acc, partial, shares,
    local_sem, send_sem, recv_sem, forget_send, forget_recv, gate_send, gate_recv, tok_send, tok_recv, sum_send, sum_recv,
):
    sp, tp = lax.axis_index("sp"), lax.axis_index("tp")
    rows = tokens_ref.shape[0]
    w_rows, width = wq_ref.shape
    block = rows * n_tp
    half = n_sp // 2

    odd = lax.rem(sp, 2)
    place = (1 - odd) * lax.div(sp, 2) + odd * (n_sp - lax.div(sp + 1, 2))

    def index_at(position):
        position = lax.rem(position + n_sp, n_sp)
        upper = lax.div(position, half)
        return (1 - upper) * 2 * position + upper * (2 * (n_sp - position) - 1)

    right, left = index_at(place + 1), index_at(place - 1)

    def view(ref, index, count, chunk):
        lanes = ref.shape[1] // 2
        return ref.at[
            pl.ds(pl.multiple_of(index * count, count), count), pl.ds(chunk * lanes, lanes)
        ]

    def hop(ring, chunk, way, step, index):
        ref, count = ((w_all, w_rows), (kv_all, block), (wo_all, w_rows))[ring]
        return pltpu.make_async_remote_copy(
            src_ref=view(ref, index, count, chunk),
            dst_ref=view(ref, index, count, chunk),
            send_sem=send_sem.at[ring, chunk, way, step],
            recv_sem=recv_sem.at[ring, chunk, way, step],
            device_id=((right, left)[way], tp),
            device_id_type=MESH,
        )

    lanes_of_ring = [(c, w, half if c == w else half - 1) for c in (0, 1) for w in (c, 1 - c)]

    def ring_start(ring):
        for chunk, way, last in lanes_of_ring:
            if last > 0:
                hop(ring, chunk, way, 1, sp).start()

    def ring_step(ring, step):
        arrived = index_at(place - step), index_at(place + step)
        for chunk, way, last in lanes_of_ring:

            @pl.when(step <= last)
            def _():
                hop(ring, chunk, way, step, arrived[way]).wait_recv()

                @pl.when(step < last)
                def _():
                    hop(ring, chunk, way, step + 1, arrived[way]).start()

        return arrived

    def ring_drain(ring):
        for chunk, way, last in lanes_of_ring:

            @pl.loop(1, last + 1)
            def _(step):
                hop(ring, chunk, way, step, sp).wait_send()

    own_rows = pl.ds(pl.multiple_of(sp * w_rows, w_rows), w_rows)
    local = [
        pltpu.make_async_copy(ref, w_all.at[own_rows, pl.ds(i * width, width)], local_sem.at[i])
        for i, ref in enumerate((wq_ref, wk_ref, wv_ref))
    ]
    local.append(pltpu.make_async_copy(wo_ref, wo_all.at[own_rows, :], local_sem.at[3]))
    for copy in local:
        copy.start()

    barrier = pltpu.get_barrier_semaphore()
    for shift in range(1, n_sp):
        pl.semaphore_signal(
            barrier, inc=1, device_id=(lax.rem(sp + shift, n_sp), tp), device_id_type=MESH
        )
    for shift in range(1, n_tp):
        pl.semaphore_signal(
            barrier, inc=1, device_id=(sp, lax.rem(tp + shift, n_tp)), device_id_type=MESH
        )

    forget_all[pl.ds(sp, 1)] = jnp.concatenate(
        [wf_ref[...].astype(F32), jnp.zeros((8 - heads, w_rows), F32)], axis=0
    )[None]
    my_rows = pl.ds(pl.multiple_of(tp * rows, rows), rows)
    normed[my_rows, :] = rms_norm(tokens_ref[...].astype(F32), gain_ref[...])
    for copy in local:
        copy.wait()
    pl.semaphore_wait(barrier, n_sp + n_tp - 2)

    def spread(ref, sends, receives):
        return [
            pltpu.make_async_remote_copy(
                src_ref=ref.at[pl.ds(sp, 1)],
                dst_ref=ref.at[pl.ds(sp, 1)],
                send_sem=sends.at[shift - 1],
                recv_sem=receives.at[shift - 1],
                device_id=(lax.rem(sp + shift, n_sp), tp),
                device_id_type=MESH,
            )
            for shift in range(1, n_sp)
        ]

    forget_copies = spread(forget_all, forget_send, forget_recv)
    for copy in forget_copies:
        copy.start()

    def tok_copy(shift):
        return pltpu.make_async_remote_copy(
            src_ref=normed.at[my_rows, :],
            dst_ref=normed.at[my_rows, :],
            send_sem=tok_send.at[shift - 1],
            recv_sem=tok_recv.at[shift - 1],
            device_id=(sp, lax.rem(tp + shift, n_tp)),
            device_id_type=MESH,
        )

    for shift in range(1, n_tp):
        tok_copy(shift).start()
    ring_start(0)

    @pl.loop(1, half)
    def _(step):
        ring_step(0, step)

    for shift in range(1, n_tp):
        tok_copy(shift).wait()
    for copy in forget_copies:
        copy.wait()

    tokens_here = normed[...]
    forget_rows = jnp.concatenate([forget_all[i] for i in range(n_sp)], axis=1).astype(BF16)
    logits = lax.dot_general(
        forget_rows, tokens_here, CONTRACT_LAST, preferred_element_type=F32
    )
    head_row = lax.broadcasted_iota(jnp.int32, (8, block), 0)
    offsets = jnp.zeros((8, block), F32)
    for h in range(heads):
        offsets = jnp.where(head_row == h, offset_ref[h], offsets)
    logits = logits + offsets + jnp.log(jnp.full((8, block), n_sp * block, F32))
    log_gates = jnp.minimum(logits, 0.0) - jnp.log1p(jnp.exp(-jnp.abs(logits)))
    row_at = lax.broadcasted_iota(jnp.int32, (block, block), 0)
    col_at = lax.broadcasted_iota(jnp.int32, (block, block), 1)
    seen = col_at <= row_at
    cum_here = jnp.dot(
        log_gates, jnp.where(row_at <= col_at, 1.0, 0.0).astype(F32),
        precision=lax.Precision.HIGHEST, preferred_element_type=F32,
    )
    gates[pl.ds(sp, 1)] = cum_here[None]
    cum_query[...] = jnp.concatenate([cum_here, jnp.zeros((LANES - 8, block), F32)], axis=0).T
    gate_copies = spread(gates, gate_send, gate_recv)
    for copy in gate_copies:
        copy.start()
    ring_step(0, half)

    ring_start(2)
    own_block = pl.ds(pl.multiple_of(sp * block, block), block)
    kv_all[own_block, :] = jnp.dot(
        tokens_here, w_all[:, width:], preferred_element_type=F32
    ).astype(BF16)
    ring_start(1)
    queries = (
        jnp.dot(tokens_here, w_all[:, :width], preferred_element_type=F32).astype(BF16).astype(F32)
        * HEAD_DIM ** (-0.5)
    )
    head_at = lax.broadcasted_iota(jnp.int32, (block, width), 1) // HEAD_DIM
    for h in range(heads):
        q_heads[h] = jnp.where(head_at == h, queries, 0.0).astype(BF16)

    def scores_of(h, index):
        key_block = kv_all[pl.ds(pl.multiple_of(index * block, block), block), :width]
        scores = lax.dot_general(
            q_heads[h], key_block, CONTRACT_LAST, preferred_element_type=F32
        )
        return scores + cum_query[:, h : h + 1] - gates[index, h : h + 1, :]

    def weighted(h, index, weights):
        value_block = kv_all[pl.ds(pl.multiple_of(index * block, block), block), width:]
        with_ones = jnp.where(head_at == h, value_block.astype(F32), 1.0).astype(BF16)
        return jnp.dot(weights.astype(BF16), with_ones, preferred_element_type=F32)

    for h in range(heads):
        scores = jnp.where(seen, scores_of(h, sp), -1e30)
        top = jnp.max(scores, axis=-1, keepdims=True)
        run_max[h] = top
        run_acc[h] = weighted(h, sp, jnp.where(seen, jnp.exp(scores - top), 0.0))

    def absorb(index):
        for h in range(heads):
            scores = scores_of(h, index)
            old = run_max[h]
            top = jnp.maximum(old, jnp.max(scores, axis=-1, keepdims=True))
            run_max[h] = top
            run_acc[h] = run_acc[h] * jnp.exp(old - top) + weighted(
                h, index, jnp.exp(scores - top)
            )

    for copy in gate_copies:
        copy.wait()

    def shift_back(count, start):
        index = sp - 1 - count
        local_cum = gates[index]
        start = start - local_cum[:, block - 1 :]
        gates[index] = local_cum + start
        return start

    lax.fori_loop(0, sp, shift_back, jnp.zeros((8, 1), F32))
    ring_step(2, 1)

    @pl.loop(1, half + 1)
    def _(step):
        first, second = ring_step(1, step)

        @pl.when(first < sp)
        def _():
            absorb(first)

        @pl.when((step < half) & (second < sp))
        def _():
            absorb(second)

        @pl.when(step < half)
        def _():
            ring_step(2, step + 1)

    attended = jnp.zeros((block, width), F32)
    for h in range(heads):
        other = ((h + 1) % heads) * HEAD_DIM
        acc = run_acc[h]
        attended = jnp.where(head_at == h, acc / acc[:, other : other + 1], attended)
    partial[...] = lax.dot_general(
        attended.astype(BF16), wo_all[...], CONTRACT_LAST, preferred_element_type=F32
    ).astype(BF16)

    def sum_copy(shift):
        peer = lax.rem(tp + shift, n_tp)
        return pltpu.make_async_remote_copy(
            src_ref=partial.at[pl.ds(pl.multiple_of(peer * rows, rows), rows), :],
            dst_ref=shares.at[shift - 1],
            send_sem=sum_send.at[shift - 1],
            recv_sem=sum_recv.at[shift - 1],
            device_id=(sp, peer),
            device_id_type=MESH,
        )

    for shift in range(1, n_tp):
        sum_copy(shift).start()
    for ring in range(3):
        ring_drain(ring)
    total = partial[my_rows, :].astype(F32)
    for shift in range(1, n_tp):
        sum_copy(shift).wait()
        total = total + shares[shift - 1].astype(F32)
    out_ref[...] = rms_norm(total, out_gain_ref[...])


def solution(mesh):
    n_sp, n_tp = mesh.shape["sp"], mesh.shape["tp"]

    def on_device(
        tokens, norm_gain, w_query, w_key, w_value, w_forget, forget_offset, w_out_t, out_gain
    ):
        rows, model = tokens.shape
        w_rows, width = w_query.shape
        heads = w_forget.shape[1]
        block = rows * n_tp
        steps = n_sp // 2 + 1
        vmem = pl.BlockSpec(memory_space=pltpu.VMEM)
        anywhere = pl.BlockSpec(memory_space=pl.ANY)
        dma = pltpu.SemaphoreType.DMA
        return pl.pallas_call(
            functools.partial(layer_kernel, n_sp, n_tp, heads),
            out_shape=jax.ShapeDtypeStruct((rows, model), BF16),
            in_specs=[
                vmem, vmem, anywhere, anywhere, anywhere, vmem,
                pl.BlockSpec(memory_space=pltpu.SMEM), anywhere, vmem,
            ],
            out_specs=vmem,
            scratch_shapes=[
                pltpu.VMEM((block, model), BF16),
                pltpu.VMEM((n_sp * w_rows, 3 * width), BF16),
                pltpu.VMEM((n_sp * w_rows, width), BF16),
                pltpu.VMEM((n_sp * block, 2 * width), BF16),
                pltpu.VMEM((n_sp, 8, w_rows), F32),
                pltpu.VMEM((n_sp, 8, block), F32),
                pltpu.VMEM((heads, block, width), BF16),
                pltpu.VMEM((block, LANES), F32),
                pltpu.VMEM((heads, block, 1), F32),
                pltpu.VMEM((heads, block, width), F32),
                pltpu.VMEM((block, model), BF16),
                pltpu.VMEM((n_tp - 1, rows, model), BF16),
                dma((4,)),
                dma((3, 2, 2, steps)),
                dma((3, 2, 2, steps)),
                dma((n_sp - 1,)),
                dma((n_sp - 1,)),
                dma((n_sp - 1,)),
                dma((n_sp - 1,)),
                dma((n_tp - 1,)),
                dma((n_tp - 1,)),
                dma((n_tp - 1,)),
                dma((n_tp - 1,)),
            ],
            compiler_params=pltpu.CompilerParams(collective_id=0, has_side_effects=True),
        )(
            tokens, norm_gain.reshape(1, model), w_query, w_key, w_value, w_forget.T,
            forget_offset, w_out_t, out_gain.reshape(1, model),
        )

    return jax.shard_map(
        on_device,
        mesh=mesh,
        in_specs=(
            P(("sp", "tp"), None),
            P(),
            P("sp", "tp"),
            P("sp", "tp"),
            P("sp", "tp"),
            P("sp", "tp"),
            P("tp"),
            P("sp", "tp"),
            P(),
        ),
        out_specs=P(("sp", "tp"), None),
        check_vma=False,
    )
```

profile of v0, /device:TPU:224, one launch (start us, length us, event | category | flops | bytes accessed | tf_op | source)
XLA Modules:
  0.0 343.3 jit_solution(2882657486742138958)
XLA Ops:
  0.0 341.7 %shard_map.91 = bf16[64,1024]{1,0:T(8,128)(2,1)} custom-call(bf16[64,1024]{1,0:T(8,128)(2,1)} %tokens_ref.1, f32[1,1024]{1,0:T(1,128)} %bitcast.3, bf16[16,256]{1,0:T(8,128)(2,1)} %wq_ref.1, bf16[16,256]{1,0:T(8,128)(2,1)} %wk_ref.1, bf16[16,256]{1,0:T(8,128)(2,1)} %wv_ref.1, bf16[4,16]{1,0:T(4,128)(2,1)} %bitcast.5, f32[4]{0:T(128)} %offset_ref.1, ...), custom_call_target="tpu_custom_call" | custom-call | tf_op jit(solution)/shard_map/pallas_call | solution.py:301
  341.7 1.6 copy.11
where the time goes:
time: 343 us
  Pallas kernels  342 us (100%)
    pallas_call x1, Pallas kernels, on_device(): pl.pallas_call(functools.partial(layer_kernel, n_sp, n_tp, heads), out_sh...  342 us

commit v1 on v0

v1 whole, which is shorter than its diff:
```python
import functools

import jax
import jax.numpy as jnp
from jax import lax
from jax.experimental import pallas as pl
from jax.experimental.pallas import tpu as pltpu
from jax.sharding import PartitionSpec as P

HEAD_DIM = 64
LANES = 128
NORM_EPS = 1e-06
NX, NC = 4, 2
MESH = pl.DeviceIdType.MESH
F32 = jnp.float32
BF16 = jnp.bfloat16
CONTRACT_LAST = (((1,), (1,)), ((), ()))


def rms_norm(floats, gain_row):
    scale_col = lax.rsqrt(jnp.mean(floats * floats, axis=-1, keepdims=True) + NORM_EPS)
    return (floats * scale_col * gain_row).astype(BF16)


def layer_kernel(
    nz, n_tp,
    tokens_ref, gain_ref, wq_ref, wk_ref, wv_ref, wf_ref, offset_ref, wo_ref, out_gain_ref,
    out_ref,
    normed, w_all, wo_all, forget_all, gates_send, gates_all, bias_all,
    kv_send, kv_all, q_send, q_recv, q_rhs, scores, run_max, run_acc, att_send, att_recv,
    local_sem, tok_send, tok_recv, wx_send, wx_recv, wz_send, wz_recv, wd_send, wd_recv,
    fx_send, fx_recv, fz_send, fz_recv, fd_send, fd_recv,
    oz_send, oz_recv, ox_send, ox_recv, oy_send, oy_recv, od_send, od_recv,
    gx_send, gx_recv, gz_send, gz_recv, kx_send, kx_recv, qx_send, qx_recv,
    kz_send, kz_recv, kd_send, kd_recv, at_send, at_recv,
):
    sp, tp = lax.axis_index("sp"), lax.axis_index("tp")
    z = lax.div(sp, NX * NC)
    x = lax.rem(lax.div(sp, NC), NX)
    c = lax.rem(sp, NC)
    rows = tokens_ref.shape[0]
    block = rows * n_tp
    half = block // 2
    model = tokens_ref.shape[1]
    width = wq_ref.shape[1]
    heads = NX
    plane_blocks = NX * NC
    far = nz // 2

    def wrap(value, size):
        return lax.rem(value + size, size)

    def at(zz, xx, cc):
        return (zz * NX + xx) * NC + cc

    def remote(src, dst, send, recv, zz, xx, cc, yy):
        return pltpu.make_async_remote_copy(
            src_ref=src, dst_ref=dst, send_sem=send, recv_sem=recv,
            device_id=(at(zz, xx, cc), yy), device_id_type=MESH,
        )

    up, down = wrap(z + 1, nz), wrap(z - 1, nz)
    other = 1 - c

    local = [
        pltpu.make_async_copy(
            ref, w_all.at[z, x, c, :, pl.ds(i * width, width)], local_sem.at[i]
        )
        for i, ref in enumerate((wq_ref, wk_ref, wv_ref))
    ]
    local.append(pltpu.make_async_copy(wo_ref, wo_all.at[tp, z, x, c], local_sem.at[3]))
    for copy in local:
        copy.start()

    barrier = pltpu.get_barrier_semaphore()
    for k in range(1, NX * n_tp):
        pl.semaphore_signal(
            barrier, inc=1, device_id_type=MESH,
            device_id=(at(z, wrap(x + k // n_tp, NX), c), wrap(tp + k % n_tp, n_tp)),
        )
    for k in range(1, nz * NC):
        cc = c if k % NC == 0 else other
        pl.semaphore_signal(
            barrier, inc=1, device_id_type=MESH,
            device_id=(at(wrap(z + k // NC, nz), x, cc), tp),
        )

    forget_all[z, x, c] = jnp.concatenate(
        [wf_ref[...].astype(F32), jnp.zeros((8 - heads, wf_ref.shape[1]), F32)], axis=0
    )
    normed[tp] = rms_norm(tokens_ref[...].astype(F32), gain_ref[...])
    for copy in local:
        copy.wait()
    pl.semaphore_wait(barrier, NX * n_tp - 1 + nz * NC - 1)

    def x_copy(ref, send, recv, dx):
        return remote(
            ref.at[z, x, c], ref.at[z, x, c], send.at[dx - 1], recv.at[dx - 1],
            z, wrap(x + dx, NX), c, tp,
        )

    def ring_subs(way, step):
        if step < far:
            return (0, 1, 2, 3)
        return (0, 1) if way == 0 else (2, 3)

    def plane_at(way, step):
        return wrap(z - step, nz) if way == 0 else wrap(z + step, nz)

    def ring_hop(ref, send, recv, way, step, sub):
        place = ref.at[plane_at(way, step - 1), wrap(x + sub, NX), c]
        return remote(
            place, place, send.at[way, step - 1, sub], recv.at[way, step - 1, sub],
            (up, down)[way], x, c, tp,
        )

    def ring_wait(ref, send, recv, way, step, sub):
        place = ref.at[plane_at(way, step), wrap(x + sub, NX), c]
        remote(
            place, place, send.at[way, step - 1, sub], recv.at[way, step - 1, sub],
            (up, down)[way], x, c, tp,
        ).wait_recv()

    def twin(ref, send, recv, way, step, sub, core):
        place = ref.at[plane_at(way, step), wrap(x + sub, NX), core]
        return remote(
            place, place, send.at[way, step, sub], recv.at[way, step, sub], z, x, other, tp
        )

    def tok_copy(dy):
        return remote(
            normed.at[tp], normed.at[tp], tok_send.at[dy - 1], tok_recv.at[dy - 1],
            z, x, c, wrap(tp + dy, n_tp),
        )

    def wo_hop(way, step):
        place = wo_all.at[tp, plane_at(way, step - 1), x, c]
        return remote(
            place, place, oz_send.at[way, step - 1], oz_recv.at[way, step - 1],
            (up, down)[way], x, c, tp,
        )

    def wo_wait(way, step):
        place = wo_all.at[tp, plane_at(way, step), x, c]
        remote(
            place, place, oz_send.at[way, step - 1], oz_recv.at[way, step - 1],
            (up, down)[way], x, c, tp,
        ).wait_recv()

    def forget_hop(way, step):
        place = forget_all.at[plane_at(way, step - 1), :, c]
        return remote(
            place, place, fz_send.at[way, step - 1], fz_recv.at[way, step - 1],
            (up, down)[way], x, c, tp,
        )

    def forget_wait(way, step):
        place = forget_all.at[plane_at(way, step), :, c]
        remote(
            place, place, fz_send.at[way, step - 1], fz_recv.at[way, step - 1],
            (up, down)[way], x, c, tp,
        ).wait_recv()

    def forget_twin(way, step, core):
        place = forget_all.at[plane_at(way, step), :, core]
        return remote(
            place, place, fd_send.at[way, step], fd_recv.at[way, step], z, x, other, tp
        )

    for dx in range(1, NX):
        x_copy(w_all, wx_send, wx_recv, dx).start()
        x_copy(forget_all, fx_send, fx_recv, dx).start()
    for way in (0, 1):
        ring_hop(w_all, wz_send, wz_recv, way, 1, 0).start()
    for dy in range(1, n_tp):
        tok_copy(dy).start()
    twin(w_all, wd_send, wd_recv, 0, 0, 0, c).start()

    for sub in range(1, NX):
        dx = NX - sub
        place = w_all.at[z, wrap(x + sub, NX), c]
        remote(
            place, place, wx_send.at[dx - 1], wx_recv.at[dx - 1], z, x, c, tp
        ).wait_recv()
        for way in (0, 1):
            ring_hop(w_all, wz_send, wz_recv, way, 1, sub).start()
        twin(w_all, wd_send, wd_recv, 0, 0, sub, c).start()
        place = forget_all.at[z, wrap(x + sub, NX), c]
        remote(
            place, place, fx_send.at[dx - 1], fx_recv.at[dx - 1], z, x, c, tp
        ).wait_recv()
    for way in (0, 1):
        forget_hop(way, 1).start()
        wo_hop(way, 1).start()
    forget_twin(0, 0, c).start()

    both = (0, 1)
    for step in range(1, far + 1):
        for sub in range(NX):
            for way in both:
                if sub not in ring_subs(way, step):
                    continue
                ring_wait(w_all, wz_send, wz_recv, way, step, sub)
                if step < far and sub in ring_subs(way, step + 1):
                    ring_hop(w_all, wz_send, wz_recv, way, step + 1, sub).start()
                twin(w_all, wd_send, wd_recv, way, step, sub, c).start()
        for way in both if step < far else (0,):
            forget_wait(way, step)
            wo_wait(way, step)
            if step + 1 < far or (step + 1 == far and way == 0):
                forget_hop(way, step + 1).start()
                wo_hop(way, step + 1).start()
            forget_twin(way, step, c).start()

    def wo_x(dx):
        place = wo_all.at[tp, :, x, c]
        return remote(
            place, place, ox_send.at[dx - 1], ox_recv.at[dx - 1], z, wrap(x + dx, NX), c, tp
        )

    def wo_y(dy):
        place = wo_all.at[tp, :, :, c]
        return remote(
            place, place, oy_send.at[dy - 1], oy_recv.at[dy - 1], z, x, c, wrap(tp + dy, n_tp)
        )

    def wo_twin(dy, core):
        place = wo_all.at[wrap(tp + dy, n_tp), :, :, core]
        return remote(place, place, od_send.at[dy], od_recv.at[dy], z, x, other, tp)

    for dy in range(1, n_tp):
        place = normed.at[wrap(tp - dy, n_tp)]
        remote(
            place, place, tok_send.at[dy - 1], tok_recv.at[dy - 1], z, x, c, tp
        ).wait_recv()
    forget_twin(0, 0, other).wait_recv()
    for step in range(1, far + 1):
        for way in both if step < far else (0,):
            forget_twin(way, step, other).wait_recv()

    tokens_here = normed[...].reshape(block, model)
    forget_rows = jnp.concatenate(
        [
            forget_all[i // plane_blocks, (i // NC) % NX, i % NC]
            for i in range(nz * plane_blocks)
        ],
        axis=1,
    ).astype(BF16)
    logits = lax.dot_general(
        forget_rows, tokens_here, CONTRACT_LAST, preferred_element_type=F32
    )
    head_row = lax.broadcasted_iota(jnp.int32, (8, block), 0)
    offsets = jnp.zeros((8, block), F32)
    for h in range(heads):
        offsets = jnp.where(head_row == h, offset_ref[h], offsets)
    n_tokens = nz * plane_blocks * block
    logits = logits + offsets + jnp.log(jnp.full((8, block), n_tokens, F32))
    log_gates = jnp.minimum(logits, 0.0) - jnp.log1p(jnp.exp(-jnp.abs(logits)))
    row_at = lax.broadcasted_iota(jnp.int32, (block, block), 0)
    col_at = lax.broadcasted_iota(jnp.int32, (block, block), 1)
    cum_here = jnp.dot(
        log_gates, jnp.where(row_at <= col_at, 1.0, 0.0).astype(F32),
        precision=lax.Precision.HIGHEST, preferred_element_type=F32,
    )
    for h in range(heads):
        gates_send[h] = cum_here[h : h + 1, :]
    gates_all[z, x, c] = gates_send[x]

    def gate_x(dx):
        hx = wrap(x + dx, NX)
        return remote(
            gates_send.at[hx], gates_all.at[z, x, c], gx_send.at[dx - 1], gx_recv.at[dx - 1],
            z, hx, c, tp,
        )

    for dx in range(1, NX):
        gate_x(dx).start()

    for step in range(0, far + 1):
        for way in both:
            if step == 0 and way == 1:
                continue
            for sub in range(NX) if step == 0 else ring_subs(way, step):
                twin(w_all, wd_send, wd_recv, way, step, sub, other).wait_recv()
    for dx in range(1, NX):
        wo_x(dx).start()

    def project(i):
        weights = w_all[:, :, :, :, i * width : (i + 1) * width].reshape(model, width)
        return jnp.dot(tokens_here, weights, preferred_element_type=F32)

    lane_at = lax.broadcasted_iota(jnp.int32, (half, LANES), 1)
    keys = project(1)
    values_t = project(2).T.astype(BF16)
    for h in range(heads):
        tile = keys[:, (h // 2) * LANES : (h // 2 + 1) * LANES]
        first, second = tile[:half], tile[half:]
        if h % 2 == 0:
            second = pltpu.roll(second, HEAD_DIM, axis=1)
        else:
            first = pltpu.roll(first, HEAD_DIM, axis=1)
        kv_send[h, :half, :] = jnp.where(lane_at < HEAD_DIM, first, second).astype(BF16)
        value_rows = values_t[h * HEAD_DIM : (h + 1) * HEAD_DIM]
        kv_send[h, half : half + HEAD_DIM, :] = value_rows[:, :half]
        kv_send[h, half + HEAD_DIM :, :] = value_rows[:, half:]

    def kv_x(dx):
        hx = wrap(x + dx, NX)
        return remote(
            kv_send.at[hx], kv_all.at[z, x, c], kx_send.at[dx - 1], kx_recv.at[dx - 1],
            z, hx, c, tp,
        )

    for dx in range(1, NX):
        kv_x(dx).start()
    kv_all[z, x, c] = kv_send[x]
    for way in both:
        ring_hop(kv_all, kz_send, kz_recv, way, 1, 0).start()
    twin(kv_all, kd_send, kd_recv, 0, 0, 0, c).start()

    queries_t = (project(0).astype(BF16).astype(F32) * HEAD_DIM ** (-0.5)).T.astype(BF16)
    for h in range(heads):
        q_send[h] = queries_t[h * HEAD_DIM : (h + 1) * HEAD_DIM]

    def q_x(dx):
        hx = wrap(x + dx, NX)
        return remote(
            q_send.at[hx], q_recv.at[x], qx_send.at[dx - 1], qx_recv.at[dx - 1], z, hx, c, tp
        )

    for dx in range(1, NX):
        q_x(dx).start()
    q_recv[x] = q_send[x]

    for dx in range(1, NX):
        place = gates_all.at[z, wrap(x - dx, NX), c]
        remote(
            place, place, gx_send.at[dx - 1], gx_recv.at[dx - 1], z, x, c, tp
        ).wait_recv()

    def gate_z(k):
        cc = c if k % NC == 0 else other
        place = gates_all.at[z, :, c]
        return remote(
            place, place, gz_send.at[k - 1], gz_recv.at[k - 1],
            wrap(z + k // NC, nz), x, cc, tp,
        )

    for k in range(1, nz * NC):
        gate_z(k).start()

    for sub in range(1, NX):
        dx = NX - sub
        place = kv_all.at[z, wrap(x + sub, NX), c]
        remote(
            place, place, kx_send.at[dx - 1], kx_recv.at[dx - 1], z, x, c, tp
        ).wait_recv()
        for way in both:
            ring_hop(kv_all, kz_send, kz_recv, way, 1, sub).start()
        twin(kv_all, kd_send, kd_recv, 0, 0, sub, c).start()

    for dx in range(1, NX):
        place = q_recv.at[wrap(x - dx, NX)]
        remote(
            place, place, qx_send.at[dx - 1], qx_recv.at[dx - 1], z, x, c, tp
        ).wait_recv()

    ones_at = lax.broadcasted_iota(jnp.int32, (LANES, block), 0)
    no_rows = jnp.zeros((HEAD_DIM, block), BF16)
    for side in (0, 1):
        picks = ((ones_at // 8) % 2 == side) & (ones_at < 6 * 8)
        picks = jnp.where(picks, 1.0, 0.0).astype(BF16)
        for i in range(NX):
            parts = [q_recv[i], no_rows] if side == 0 else [no_rows, q_recv[i]]
            q_rhs[i, side] = jnp.concatenate(parts + [picks], axis=0)

    for k in range(1, nz * NC):
        cc = c if k % NC == 0 else other
        place = gates_all.at[wrap(z - k // NC, nz), :, cc]
        remote(
            place, place, gz_send.at[k - 1], gz_recv.at[k - 1], z, x, other, tp
        ).wait_recv()

    n_blocks = nz * plane_blocks
    gate_rows = gates_all[...].reshape(n_blocks, block)
    mine = z * plane_blocks
    row_block = lax.broadcasted_iota(jnp.int32, (n_blocks, n_blocks), 0)
    col_block = lax.broadcasted_iota(jnp.int32, (n_blocks, n_blocks), 1)
    behind = (col_block >= row_block) & (col_block < mine)
    ahead = (col_block < row_block) & (col_block >= mine)
    steps_between = jnp.where(ahead, 1.0, 0.0) - jnp.where(behind, 1.0, 0.0)
    starts = jnp.dot(
        steps_between, gate_rows[:, half:], precision=lax.Precision.HIGHEST,
        preferred_element_type=F32,
    )[:, half - 1 :]
    bias = -(starts + gate_rows)
    bias_high = bias.astype(BF16).astype(F32)
    bias_rest = bias - bias_high
    bias_mid = bias_rest.astype(BF16).astype(F32)
    bias_low = bias_rest - bias_mid
    no_bias = jnp.zeros((LANES - 6 * plane_blocks, LANES), F32)
    for zz in range(nz):
        here = slice(zz * plane_blocks, (zz + 1) * plane_blocks)
        stack = []
        for part in (bias_high, bias_mid, bias_low):
            stack += [part[here, :half], part[here, half:]]
        bias_all[zz] = jnp.concatenate(stack + [no_bias], axis=0).T.astype(BF16)

    lane_block = lax.broadcasted_iota(jnp.int32, (8, LANES), 1) % 8
    ones_rows = jnp.ones((16, plane_blocks * half), BF16)

    def attend(plane, own):
        key_rows = kv_all[plane, :, :, :half, :].reshape(plane_blocks * half, LANES)
        bias_cols = bias_all[plane]
        masks = [
            jnp.where(lane_block == b, 1.0, 0.0)[:1].astype(BF16) for b in range(plane_blocks)
        ]
        bias_tiles = jnp.concatenate([bias_cols * mask for mask in masks], axis=0)
        left = jnp.concatenate([key_rows, bias_tiles], axis=1)

        def score(i):
            tops = []
            for side in (0, 1):
                s = jnp.dot(left, q_rhs[i, side], preferred_element_type=F32)
                if own:
                    row = lax.broadcasted_iota(jnp.int32, s.shape, 0)
                    key_at = (row // half) * block + side * half + row % half
                    query_at = lax.broadcasted_iota(jnp.int32, s.shape, 1) + (
                        (i * NC + c) * block
                    )
                    s = jnp.where(key_at <= query_at, s, -1e30)
                scores[i, side] = s
                tops.append(jnp.max(s, axis=0, keepdims=True))
            return jnp.maximum(tops[0], tops[1])

        def absorb(i, top):
            if own:
                total = jnp.zeros((HEAD_DIM + 16, block), F32)
            else:
                old = run_max[i]
                top = jnp.maximum(old, top)
                total = run_acc[i] * jnp.exp(old - top)
            run_max[i] = top
            for side in (0, 1):
                weights = jnp.exp(scores[i, side] - top).astype(BF16)
                lo = half + side * HEAD_DIM
                value_cols = jnp.concatenate(
                    [
                        kv_all[plane, b // NC, b % NC, lo : lo + HEAD_DIM, :]
                        for b in range(plane_blocks)
                    ],
                    axis=1,
                )
                value_cols = jnp.concatenate([value_cols, ones_rows], axis=0)
                total = total + jnp.dot(value_cols, weights, preferred_element_type=F32)
            run_acc[i] = total

        tops = [score(0)]
        for i in range(NX):
            if i + 1 < NX:
                tops.append(score(i + 1))
            absorb(i, tops[i])

    for sub in range(NX):
        twin(kv_all, kd_send, kd_recv, 0, 0, sub, other).wait_recv()
    attend(z, True)

    for dx in range(1, NX):
        place = wo_all.at[tp, :, wrap(x - dx, NX), c]
        remote(
            place, place, ox_send.at[dx - 1], ox_recv.at[dx - 1], z, x, c, tp
        ).wait_recv()
    for dy in range(1, n_tp):
        wo_y(dy).start()
    wo_twin(0, c).start()

    def kv_step(step):
        last = step == far
        for sub in range(NX):
            for way in both:
                if sub not in ring_subs(way, step):
                    continue
                ring_wait(kv_all, kz_send, kz_recv, way, step, sub)
                if not last and sub in ring_subs(way, step + 1):
                    ring_hop(kv_all, kz_send, kz_recv, way, step + 1, sub).start()
                twin(kv_all, kd_send, kd_recv, way, step, sub, c).start()

    def maybe_attend(plane):
        @pl.when(plane < z)
        def _():
            attend(plane, False)

    for step in range(1, far + 1):
        kv_step(step)
        if step > 1:
            maybe_attend(plane_at(1, step - 1))
        for way in both:
            for sub in ring_subs(way, step):
                twin(kv_all, kd_send, kd_recv, way, step, sub, other).wait_recv()
        maybe_attend(plane_at(0, step))

    for dy in range(1, n_tp):
        place = wo_all.at[wrap(tp - dy, n_tp), :, :, c]
        remote(
            place, place, oy_send.at[dy - 1], oy_recv.at[dy - 1], z, x, c, tp
        ).wait_recv()
        wo_twin(n_tp - dy, c).start()

    my_head = tp * NX + x
    odd = lax.rem(x, 2)
    row_in = lax.broadcasted_iota(jnp.int32, (2 * HEAD_DIM, block), 0) // HEAD_DIM

    def att_copy(i, dy):
        yy = wrap(tp + dy, n_tp)
        return remote(
            att_send.at[i, pl.ds(pl.multiple_of(yy * rows, rows), rows), :],
            att_recv.at[my_head], at_send.at[i, dy], at_recv.at[my_head],
            z, i, c, yy,
        )

    for i in range(NX):
        acc = run_acc[i]
        att = acc[:HEAD_DIM] / acc[HEAD_DIM : HEAD_DIM + 1]
        att = jnp.where(row_in == odd, jnp.concatenate([att, att], axis=0), 0.0)
        att_send[i] = att.T.astype(BF16)
        for dy in range(n_tp):
            if dy == 0:

                @pl.when(x != i)
                def _():
                    att_copy(i, dy).start()
            else:
                att_copy(i, dy).start()
    att_recv[my_head] = att_send[x, pl.ds(pl.multiple_of(tp * rows, rows), rows), :]

    for dy in range(n_tp):
        wo_twin(dy, other).wait_recv()
    for k in range(1, NX * n_tp):
        source = wrap(my_head + k, NX * n_tp)
        place = att_recv.at[source]
        remote(place, place, at_send.at[0, 0], at_recv.at[source], z, x, c, tp).wait_recv()

    projected = jnp.zeros((rows, model), F32)
    for y in range(n_tp):
        pieces = []
        for pair in range(NX // 2):
            even = y * NX + 2 * pair
            pieces.append(att_recv[even] + att_recv[even + 1])
        columns = jnp.concatenate(pieces, axis=1)
        projected = projected + lax.dot_general(
            columns, wo_all[y].reshape(model, width), CONTRACT_LAST, preferred_element_type=F32
        )
    out_ref[...] = rms_norm(projected, out_gain_ref[...])

    for d in range(1, NX):
        x_copy(w_all, wx_send, wx_recv, d).wait_send()
        x_copy(forget_all, fx_send, fx_recv, d).wait_send()
        wo_x(d).wait_send()
        gate_x(d).wait_send()
        kv_x(d).wait_send()
        q_x(d).wait_send()
    for d in range(1, n_tp):
        tok_copy(d).wait_send()
        wo_y(d).wait_send()
    for d in range(n_tp):
        wo_twin(d, c).wait_send()
    for k in range(1, nz * NC):
        gate_z(k).wait_send()
    for step in range(0, far + 1):
        for way in both:
            if step == 0 and way == 1:
                continue
            for sub in range(NX) if step == 0 else ring_subs(way, step):
                twin(w_all, wd_send, wd_recv, way, step, sub, c).wait_send()
                twin(kv_all, kd_send, kd_recv, way, step, sub, c).wait_send()
                if step > 0:
                    ring_hop(w_all, wz_send, wz_recv, way, step, sub).wait_send()
                    ring_hop(kv_all, kz_send, kz_recv, way, step, sub).wait_send()
            if step < far or way == 0:
                forget_twin(way, step, c).wait_send()
                if step > 0:
                    forget_hop(way, step).wait_send()
                    wo_hop(way, step).wait_send()
    for i in range(NX):
        for dy in range(n_tp):
            if dy == 0:

                @pl.when(x != i)
                def _():
                    att_copy(i, dy).wait_send()
            else:
                att_copy(i, dy).wait_send()


def solution(mesh):
    n_sp, n_tp = mesh.shape["sp"], mesh.shape["tp"]
    nz = n_sp // (NX * NC)

    def on_device(
        tokens, norm_gain, w_query, w_key, w_value, w_forget, forget_offset, w_out_t, out_gain
    ):
        rows, model = tokens.shape
        w_rows, width = w_query.shape
        heads = w_forget.shape[1]
        block = rows * n_tp
        half = block // 2
        far = nz // 2
        vmem = pl.BlockSpec(memory_space=pltpu.VMEM)
        anywhere = pl.BlockSpec(memory_space=pl.ANY)
        dma = pltpu.SemaphoreType.DMA

        def pair(*shape):
            return [dma(shape), dma(shape)]

        return pl.pallas_call(
            functools.partial(layer_kernel, nz, n_tp),
            out_shape=jax.ShapeDtypeStruct((rows, model), BF16),
            in_specs=[
                vmem, vmem, anywhere, anywhere, anywhere, vmem,
                pl.BlockSpec(memory_space=pltpu.SMEM), anywhere, vmem,
            ],
            out_specs=vmem,
            scratch_shapes=[
                pltpu.VMEM((n_tp, rows, model), BF16),
                pltpu.VMEM((nz, NX, NC, w_rows, 3 * width), BF16),
                pltpu.VMEM((n_tp, nz, NX, NC, w_rows, width), BF16),
                pltpu.VMEM((nz, NX, NC, 8, w_rows), F32),
                pltpu.VMEM((heads, 1, block), F32),
                pltpu.VMEM((nz, NX, NC, 1, block), F32),
                pltpu.VMEM((nz, LANES, LANES), BF16),
                pltpu.VMEM((heads, block, LANES), BF16),
                pltpu.VMEM((nz, NX, NC, block, LANES), BF16),
                pltpu.VMEM((heads, HEAD_DIM, block), BF16),
                pltpu.VMEM((NX, HEAD_DIM, block), BF16),
                pltpu.VMEM((NX, 2, block, block), BF16),
                pltpu.VMEM((NX, 2, NX * NC * half, block), F32),
                pltpu.VMEM((NX, 1, block), F32),
                pltpu.VMEM((NX, HEAD_DIM + 16, block), F32),
                pltpu.VMEM((NX, block, LANES), BF16),
                pltpu.VMEM((NX * n_tp, rows, LANES), BF16),
                dma((4,)),
                *pair(n_tp - 1),
                *pair(NX - 1),
                *pair(2, far, NX),
                *pair(2, far + 1, NX),
                *pair(NX - 1),
                *pair(2, far),
                *pair(2, far + 1),
                *pair(2, far),
                *pair(NX - 1),
                *pair(n_tp - 1),
                *pair(n_tp),
                *pair(NX - 1),
                *pair(nz * NC - 1),
                *pair(NX - 1),
                *pair(NX - 1),
                *pair(2, far, NX),
                *pair(2, far + 1, NX),
                dma((NX, n_tp)),
                dma((NX * n_tp,)),
            ],
            compiler_params=pltpu.CompilerParams(collective_id=0, has_side_effects=True),
        )(
            tokens, norm_gain.reshape(1, model), w_query, w_key, w_value, w_forget.T,
            forget_offset, w_out_t, out_gain.reshape(1, model),
        )

    return jax.shard_map(
        on_device,
        mesh=mesh,
        in_specs=(
            P(("sp", "tp"), None),
            P(),
            P("sp", "tp"),
            P("sp", "tp"),
            P("sp", "tp"),
            P("sp", "tp"),
            P("tp"),
            P("sp", "tp"),
            P(),
        ),
        out_specs=P(("sp", "tp"), None),
        check_vma=False,
    )
```

time: 343 us -> 76.1 us (0.22)
  Pallas kernels: 342 us -> 73.5 us
    pallas_call x1, Pallas kernels: 342 us -> 73.5 us  [on_device(): pl.pallas_call(functools.partial(layer_kernel, nz, n_tp), out_shape=jax.S...]
where the time goes in v1:
time: 76.1 us; the launch traced here: 75 us
  Pallas kernels  73.5 us (97%)
  local copies, waits for them, and re-layouts  1.57 us (2%)
    pallas_call x1, Pallas kernels, on_device(): pl.pallas_call(functools.partial(layer_kernel, nz, n_tp), out_shape=jax.S...  73.5 us
    unnamed x1, local copies, waits for them, and re-layouts  1.57 us

profile of v1, /device:TPU:224, one launch (start us, length us, event | category | flops | bytes accessed | tf_op | source)
XLA Modules:
  0.0 75.0 jit_solution(6607123492967690205)
XLA Ops:
  0.0 73.5 %shard_map.91 = bf16[64,1024]{1,0:T(8,128)(2,1)} custom-call(bf16[64,1024]{1,0:T(8,128)(2,1)} %tokens_ref.1, f32[1,1024]{1,0:T(1,128)} %bitcast.3, bf16[16,256]{1,0:T(8,128)(2,1)} %wq_ref.1, bf16[16,256]{1,0:T(8,128)(2,1)} %wk_ref.1, bf16[16,256]{1,0:T(8,128)(2,1)} %wv_ref.1, bf16[4,16]{1,0:T(4,128)(2,1)} %bitcast.5, f32[4]{0:T(128)} %offset_ref.1, ...), custom_call_target="tpu_custom_call" | custom-call | tf_op jit(solution)/shard_map/pallas_call | solution.py:615
  73.5 1.6 %copy.11 = bf16[64,1024]{1,0:T(8,128)(2,1)} copy(bf16[64,1024]{1,0:T(8,128)(2,1)} %shard_map.91) | data formatting | bytes 262144

commit v2 on v1

v2 whole, which is shorter than its diff:
```python
import functools

import jax
import jax.numpy as jnp
from jax import lax
from jax.experimental import pallas as pl
from jax.experimental.pallas import tpu as pltpu
from jax.sharding import PartitionSpec as P

HEAD_DIM = 64
LANES = 128
NORM_EPS = 1e-06
NX, NC = 4, 2
CHUNK, LAG = 4, 4
MESH = pl.DeviceIdType.MESH
F32 = jnp.float32
BF16 = jnp.bfloat16
CONTRACT_LAST = (((1,), (1,)), ((), ()))


def rms_norm(floats, gain_row):
    scale_col = lax.rsqrt(jnp.mean(floats * floats, axis=-1, keepdims=True) + NORM_EPS)
    return (floats * scale_col * gain_row).astype(BF16)


def layer_kernel(
    nz, n_tp,
    tokens_ref, gain_ref, wq_ref, wk_ref, wv_ref, wf_ref, offset_ref, wo_ref, out_gain_ref,
    out_ref,
    normed, w_kv, w_q, wo_all, forget_all, gates_send, gates_all, bias_all,
    kv_send, kv_all, q_send, q_recv, q_rhs, left, scores, run_max, run_acc, att_send, att_recv,
    local_sem, tok_send, tok_recv, wz_send, wz_recv, wx_send, wx_recv, wd_send, wd_recv,
    fz_send, fz_recv, fx_send, fx_recv, fd_send, fd_recv,
    oz_send, oz_recv, ox_send, ox_recv, oy_send, oy_recv, od_send, od_recv,
    gx_send, gx_recv, gz_send, gz_recv, kx_send, kx_recv, qx_send, qx_recv,
    kz_send, kz_recv, kd_send, kd_recv, at_send, at_recv,
):
    sp, tp = lax.axis_index("sp"), lax.axis_index("tp")
    z = lax.div(sp, NX * NC)
    x = lax.rem(lax.div(sp, NC), NX)
    c = lax.rem(sp, NC)
    rows = tokens_ref.shape[0]
    block = rows * n_tp
    half = block // 2
    model = tokens_ref.shape[1]
    width = wq_ref.shape[1]
    heads = NX
    plane_blocks = NX * NC
    far = nz // 2

    def wrap(value, size):
        return lax.rem(value + size, size)

    def at(zz, xx, cc):
        return (zz * NX + xx) * NC + cc

    def remote(src, dst, send, recv, zz, xx, cc, yy):
        return pltpu.make_async_remote_copy(
            src_ref=src, dst_ref=dst, send_sem=send, recv_sem=recv,
            device_id=(at(zz, xx, cc), yy), device_id_type=MESH,
        )

    up, down = wrap(z + 1, nz), wrap(z - 1, nz)
    other = 1 - c

    weights = (w_kv, w_q)
    local = [
        pltpu.make_async_copy(
            ref, place.at[z, x, c, :, pl.ds(i * width, width)], local_sem.at[n]
        )
        for n, (ref, place, i) in enumerate(
            ((wk_ref, w_kv, 0), (wv_ref, w_kv, 1), (wq_ref, w_q, 0))
        )
    ]
    local.append(pltpu.make_async_copy(wo_ref, wo_all.at[tp, z, x, c], local_sem.at[3]))
    for copy in local:
        copy.start()

    barrier = pltpu.get_barrier_semaphore()
    near = [(at(z, wrap(x + dx, NX), c), tp) for dx in range(1, NX)]
    near += [(sp, wrap(tp + dy, n_tp)) for dy in range(1, n_tp)]
    near += [(at(wrap(z + dz, nz), x, c), tp) for dz in range(1, nz)]
    near += [(at(z, x, other), tp)]
    for device in near:
        pl.semaphore_signal(barrier, inc=1, device_id_type=MESH, device_id=device)

    forget_all[z, x, c] = jnp.concatenate(
        [wf_ref[...].astype(F32), jnp.zeros((8 - heads, wf_ref.shape[1]), F32)], axis=0
    )
    normed[tp] = rms_norm(tokens_ref[...].astype(F32), gain_ref[...])
    for copy in local:
        copy.wait()
    pl.semaphore_wait(barrier, len(near))

    def w_place(a, k, dx, core):
        return weights[a].at[wrap(z - k, nz), wrap(x + dx, NX), core]

    def w_z(a, k):
        place = w_place(a, 0, 0, c)
        return remote(
            place, place, wz_send.at[a, k], wz_recv.at[a, k], wrap(z + k, nz), x, c, tp
        )

    def w_x(a, k, dx):
        place = w_place(a, k, 0, c)
        return remote(
            place, place, wx_send.at[a, k, dx], wx_recv.at[a, k, dx],
            z, wrap(x + dx, NX), c, tp,
        )

    def w_twin(a, k, dx, core):
        place = w_place(a, k, dx, core)
        return remote(
            place, place, wd_send.at[a, k, dx], wd_recv.at[a, k, dx], z, x, other, tp
        )

    def w_onward(a, k):
        for dx in (2, 1, 3):
            w_x(a, k, dx).start()
        w_twin(a, k, 0, c).start()

    def nearest(n):
        return jnp.where(lax.rem(n, 2) == 1, lax.div(n + 1, 2), nz - lax.div(n, 2))

    def w_from_z(a):
        w_onward(a, 0)

        @pl.loop(1, nz)
        def _(n):
            k = nearest(n)
            place = w_place(a, k, 0, c)
            remote(
                place, place, wz_send.at[a, k], wz_recv.at[a, k], up, x, c, tp
            ).wait_recv()
            w_onward(a, k)

    def w_from_x(a):
        @pl.loop(0, nz)
        def _(n):
            k = jnp.where(n == 0, 0, nearest(n))
            for dx in (1, 3, 2):
                place = w_place(a, k, NX - dx, c)
                remote(
                    place, place, wx_send.at[a, k, dx], wx_recv.at[a, k, dx],
                    z, wrap(x + 1, NX), c, tp,
                ).wait_recv()
                w_twin(a, k, NX - dx, c).start()

    def w_from_twin(a):
        @pl.loop(0, nz)
        def _(k):
            for dx in range(NX):
                w_twin(a, k, dx, other).wait_recv()

    def ring_subs(way, step):
        if step < far:
            return (0, 1, 2, 3)
        return (0, 1) if way == 0 else (2, 3)

    def plane_at(way, step):
        return wrap(z - step, nz) if way == 0 else wrap(z + step, nz)

    def ring_hop(ref, send, recv, way, step, sub):
        place = ref.at[plane_at(way, step - 1), wrap(x + sub, NX), c]
        return remote(
            place, place, send.at[way, step - 1, sub], recv.at[way, step - 1, sub],
            (up, down)[way], x, c, tp,
        )

    def ring_wait(ref, send, recv, way, step, sub):
        place = ref.at[plane_at(way, step), wrap(x + sub, NX), c]
        remote(
            place, place, send.at[way, step - 1, sub], recv.at[way, step - 1, sub],
            (up, down)[way], x, c, tp,
        ).wait_recv()

    def twin(ref, send, recv, way, step, sub, core):
        place = ref.at[plane_at(way, step), wrap(x + sub, NX), core]
        return remote(
            place, place, send.at[way, step, sub], recv.at[way, step, sub], z, x, other, tp
        )

    def tok_copy(dy):
        return remote(
            normed.at[tp], normed.at[tp], tok_send.at[dy - 1], tok_recv.at[dy - 1],
            z, x, c, wrap(tp + dy, n_tp),
        )

    def forget_z(k):
        place = forget_all.at[z, x, c]
        return remote(
            place, place, fz_send.at[k - 1], fz_recv.at[k - 1], wrap(z + k, nz), x, c, tp
        )

    def forget_x(dx):
        place = forget_all.at[:, x, c]
        return remote(
            place, place, fx_send.at[dx - 1], fx_recv.at[dx - 1], z, wrap(x + dx, NX), c, tp
        )

    def forget_twin(core):
        place = forget_all.at[:, :, core]
        return remote(place, place, fd_send.at[0], fd_recv.at[0], z, x, other, tp)

    def wo_z(k):
        place = wo_all.at[tp, z, x, c]
        return remote(
            place, place, oz_send.at[k - 1], oz_recv.at[k - 1], wrap(z + k, nz), x, c, tp
        )

    def wo_x(dx):
        place = wo_all.at[tp, :, x, c]
        return remote(
            place, place, ox_send.at[dx - 1], ox_recv.at[dx - 1], z, wrap(x + dx, NX), c, tp
        )

    def wo_y(dy):
        place = wo_all.at[tp, :, :, c]
        return remote(
            place, place, oy_send.at[dy - 1], oy_recv.at[dy - 1], z, x, c, wrap(tp + dy, n_tp)
        )

    def wo_twin(dy, core):
        place = wo_all.at[wrap(tp + dy, n_tp), :, :, core]
        return remote(place, place, od_send.at[dy], od_recv.at[dy], z, x, other, tp)

    both = (0, 1)
    far_first = sorted(range(1, nz), key=lambda k: -min(k, nz - k))
    for k in far_first:
        w_z(0, k).start()
    for dy in range(1, n_tp):
        tok_copy(dy).start()
    for k in far_first:
        forget_z(k).start()
    for k in far_first:
        w_z(1, k).start()
    for k in far_first:
        wo_z(k).start()

    w_from_z(0)
    for k in range(1, nz):
        place = forget_all.at[wrap(z - k, nz), x, c]
        remote(place, place, fz_send.at[k - 1], fz_recv.at[k - 1], up, x, c, tp).wait_recv()
    for dx in range(1, NX):
        forget_x(dx).start()
    w_from_z(1)
    w_from_x(0)
    for dx in range(1, NX):
        place = forget_all.at[:, wrap(x - dx, NX), c]
        remote(
            place, place, fx_send.at[dx - 1], fx_recv.at[dx - 1], z, x, c, tp
        ).wait_recv()
    forget_twin(c).start()
    for dy in range(1, n_tp):
        place = normed.at[wrap(tp - dy, n_tp)]
        remote(
            place, place, tok_send.at[dy - 1], tok_recv.at[dy - 1], z, x, c, tp
        ).wait_recv()
    tokens_here = normed[...].reshape(block, model)
    forget_twin(other).wait_recv()
    forget_rows = jnp.concatenate(
        [
            forget_all[i // plane_blocks, (i // NC) % NX, i % NC]
            for i in range(nz * plane_blocks)
        ],
        axis=1,
    ).astype(BF16)
    logits = lax.dot_general(
        forget_rows, tokens_here, CONTRACT_LAST, preferred_element_type=F32
    )
    head_row = lax.broadcasted_iota(jnp.int32, (8, block), 0)
    offsets = jnp.zeros((8, block), F32)
    for h in range(heads):
        offsets = jnp.where(head_row == h, offset_ref[h], offsets)
    n_tokens = nz * plane_blocks * block
    logits = logits + offsets + jnp.log(jnp.full((8, block), n_tokens, F32))
    log_gates = jnp.minimum(logits, 0.0) - jnp.log1p(jnp.exp(-jnp.abs(logits)))
    row_at = lax.broadcasted_iota(jnp.int32, (block, block), 0)
    col_at = lax.broadcasted_iota(jnp.int32, (block, block), 1)
    cum_here = jnp.dot(
        log_gates, jnp.where(row_at <= col_at, 1.0, 0.0).astype(F32),
        precision=lax.Precision.HIGHEST, preferred_element_type=F32,
    )
    for h in range(heads):
        gates_send[h] = cum_here[h : h + 1, :]
    gates_all[z, x, c] = gates_send[x]

    def gate_x(dx):
        hx = wrap(x + dx, NX)
        return remote(
            gates_send.at[hx], gates_all.at[z, x, c], gx_send.at[dx - 1], gx_recv.at[dx - 1],
            z, hx, c, tp,
        )

    for dx in range(1, NX):
        gate_x(dx).start()

    w_from_twin(0)

    def project(ref, i):
        columns = ref[:, :, :, :, i * width : (i + 1) * width].reshape(model, width)
        return jnp.dot(tokens_here, columns, preferred_element_type=F32)

    lane_at = lax.broadcasted_iota(jnp.int32, (half, LANES), 1)
    keys = project(w_kv, 0)
    values_t = project(w_kv, 1).T.astype(BF16)
    for h in range(heads):
        tile = keys[:, (h // 2) * LANES : (h // 2 + 1) * LANES]
        first, second = tile[:half], tile[half:]
        if h % 2 == 0:
            second = pltpu.roll(second, HEAD_DIM, axis=1)
        else:
            first = pltpu.roll(first, HEAD_DIM, axis=1)
        kv_send[h, :half, :] = jnp.where(lane_at < HEAD_DIM, first, second).astype(BF16)
        value_rows = values_t[h * HEAD_DIM : (h + 1) * HEAD_DIM]
        kv_send[h, half : half + HEAD_DIM, :] = value_rows[:, :half]
        kv_send[h, half + HEAD_DIM :, :] = value_rows[:, half:]

    def kv_x(dx):
        hx = wrap(x + dx, NX)
        return remote(
            kv_send.at[hx], kv_all.at[z, x, c], kx_send.at[dx - 1], kx_recv.at[dx - 1],
            z, hx, c, tp,
        )

    for dx in range(1, NX):
        kv_x(dx).start()
    kv_all[z, x, c] = kv_send[x]
    for way in both:
        ring_hop(kv_all, kz_send, kz_recv, way, 1, 0).start()
    twin(kv_all, kd_send, kd_recv, 0, 0, 0, c).start()

    for dx in range(1, NX):
        place = gates_all.at[z, wrap(x - dx, NX), c]
        remote(
            place, place, gx_send.at[dx - 1], gx_recv.at[dx - 1], z, x, c, tp
        ).wait_recv()

    def gate_z(k):
        cc = c if k % NC == 0 else other
        place = gates_all.at[z, :, c]
        return remote(
            place, place, gz_send.at[k - 1], gz_recv.at[k - 1],
            wrap(z + k // NC, nz), x, cc, tp,
        )

    for k in range(1, nz * NC):
        gate_z(k).start()

    w_from_x(1)
    w_from_twin(1)
    queries_t = (project(w_q, 0).astype(BF16).astype(F32) * HEAD_DIM ** (-0.5)).T.astype(BF16)
    for h in range(heads):
        q_send[h] = queries_t[h * HEAD_DIM : (h + 1) * HEAD_DIM]

    def q_x(dx):
        hx = wrap(x + dx, NX)
        return remote(
            q_send.at[hx], q_recv.at[x], qx_send.at[dx - 1], qx_recv.at[dx - 1], z, hx, c, tp
        )

    for dx in range(1, NX):
        q_x(dx).start()
    q_recv[x] = q_send[x]

    for sub in range(1, NX):
        dx = NX - sub
        place = kv_all.at[z, wrap(x + sub, NX), c]
        remote(
            place, place, kx_send.at[dx - 1], kx_recv.at[dx - 1], z, x, c, tp
        ).wait_recv()
        for way in both:
            ring_hop(kv_all, kz_send, kz_recv, way, 1, sub).start()
        twin(kv_all, kd_send, kd_recv, 0, 0, sub, c).start()

    for dx in range(1, NX):
        place = q_recv.at[wrap(x - dx, NX)]
        remote(
            place, place, qx_send.at[dx - 1], qx_recv.at[dx - 1], z, x, c, tp
        ).wait_recv()

    for k in range(1, nz):
        place = wo_all.at[tp, wrap(z - k, nz), x, c]
        remote(place, place, oz_send.at[k - 1], oz_recv.at[k - 1], up, x, c, tp).wait_recv()
    for dx in range(1, NX):
        wo_x(dx).start()
    ones_at = lax.broadcasted_iota(jnp.int32, (LANES, block), 0)
    no_rows = jnp.zeros((HEAD_DIM, block), BF16)
    for side in (0, 1):
        picks = ((ones_at // 8) % 2 == side) & (ones_at < 6 * 8)
        picks = jnp.where(picks, 1.0, 0.0).astype(BF16)
        for i in range(NX):
            parts = [q_recv[i], no_rows] if side == 0 else [no_rows, q_recv[i]]
            q_rhs[i, side] = jnp.concatenate(parts + [picks], axis=0)

    for k in range(1, nz * NC):
        cc = c if k % NC == 0 else other
        place = gates_all.at[wrap(z - k // NC, nz), :, cc]
        remote(
            place, place, gz_send.at[k - 1], gz_recv.at[k - 1], z, x, other, tp
        ).wait_recv()

    n_blocks = nz * plane_blocks
    gate_rows = gates_all[...].reshape(n_blocks, block)
    mine = z * plane_blocks
    row_block = lax.broadcasted_iota(jnp.int32, (n_blocks, n_blocks), 0)
    col_block = lax.broadcasted_iota(jnp.int32, (n_blocks, n_blocks), 1)
    behind = (col_block >= row_block) & (col_block < mine)
    ahead = (col_block < row_block) & (col_block >= mine)
    steps_between = jnp.where(ahead, 1.0, 0.0) - jnp.where(behind, 1.0, 0.0)
    starts = jnp.dot(
        steps_between, gate_rows[:, half:], precision=lax.Precision.HIGHEST,
        preferred_element_type=F32,
    )[:, half - 1 :]
    bias = -(starts + gate_rows)
    bias_high = bias.astype(BF16).astype(F32)
    bias_rest = bias - bias_high
    bias_mid = bias_rest.astype(BF16).astype(F32)
    bias_low = bias_rest - bias_mid
    no_bias = jnp.zeros((LANES - 6 * plane_blocks, LANES), F32)
    for zz in range(nz):
        here = slice(zz * plane_blocks, (zz + 1) * plane_blocks)
        stack = []
        for part in (bias_high, bias_mid, bias_low):
            stack += [part[here, :half], part[here, half:]]
        bias_all[zz] = jnp.concatenate(stack + [no_bias], axis=0).T.astype(BF16)

    lane_block = lax.broadcasted_iota(jnp.int32, (8, LANES), 1) % 8
    ones_rows = jnp.ones((16, CHUNK * half), BF16)

    def attend(plane, own):
        key_rows = kv_all[plane, :, :, :half, :].reshape(plane_blocks * half, LANES)
        bias_cols = bias_all[plane]
        masks = [
            jnp.where(lane_block == b, 1.0, 0.0)[:1].astype(BF16) for b in range(plane_blocks)
        ]
        bias_tiles = jnp.concatenate([bias_cols * mask for mask in masks], axis=0)
        left[...] = jnp.concatenate([key_rows, bias_tiles], axis=1)

        def score(i, side, b0):
            span = slice(b0 * half, (b0 + CHUNK) * half)
            s = jnp.dot(left[span, :], q_rhs[i, side], preferred_element_type=F32)
            if own:
                row = lax.broadcasted_iota(jnp.int32, s.shape, 0)
                key_at = (b0 + row // half) * block + side * half + row % half
                query_at = lax.broadcasted_iota(jnp.int32, s.shape, 1) + (
                    (i * NC + c) * block
                )
                s = jnp.where(key_at <= query_at, s, -1e30)
            scores[i, side, span, :] = s
            return jnp.max(s, axis=0, keepdims=True)

        def absorb(i, side, b0, top):
            if own and side == 0 and b0 == 0:
                total = jnp.zeros((HEAD_DIM + 16, block), F32)
            else:
                old = run_max[i]
                top = jnp.maximum(old, top)
                total = run_acc[i] * jnp.exp(old - top)
            run_max[i] = top
            span = slice(b0 * half, (b0 + CHUNK) * half)
            weights = jnp.exp(scores[i, side, span, :] - top).astype(BF16)
            lo = half + side * HEAD_DIM
            value_cols = jnp.concatenate(
                [
                    kv_all[plane, b // NC, b % NC, lo : lo + HEAD_DIM, :]
                    for b in range(b0, b0 + CHUNK)
                ],
                axis=1,
            )
            value_cols = jnp.concatenate([value_cols, ones_rows], axis=0)
            run_acc[i] = total + jnp.dot(value_cols, weights, preferred_element_type=F32)

        chunks = [
            (i, side, b0)
            for i in range(NX) for side in (0, 1) for b0 in range(0, plane_blocks, CHUNK)
        ]
        tops = []
        for n in range(len(chunks) + LAG):
            if n < len(chunks):
                tops.append(score(*chunks[n]))
            if n >= LAG:
                absorb(*chunks[n - LAG], tops[n - LAG])

    for sub in range(NX):
        twin(kv_all, kd_send, kd_recv, 0, 0, sub, other).wait_recv()
    attend(z, True)

    for dx in range(1, NX):
        place = wo_all.at[tp, :, wrap(x - dx, NX), c]
        remote(
            place, place, ox_send.at[dx - 1], ox_recv.at[dx - 1], z, x, c, tp
        ).wait_recv()
    for dy in range(1, n_tp):
        wo_y(dy).start()
    wo_twin(0, c).start()

    def kv_step(step):
        for sub in range(NX):
            for way in both:
                whole = (sub < NX // 2) == (way == 0)

                def receive():
                    ring_wait(kv_all, kz_send, kz_recv, way, step, sub)
                    twin(kv_all, kd_send, kd_recv, way, step, sub, c).start()

                    @pl.when(step + (0 if whole else 1) < far)
                    def _():
                        ring_hop(kv_all, kz_send, kz_recv, way, step + 1, sub).start()

                if whole:
                    receive()
                else:
                    pl.when(step < far)(receive)

    def twin_step(step):
        for sub in range(NX):
            for way in both:

                def receive():
                    twin(kv_all, kd_send, kd_recv, way, step, sub, other).wait_recv()

                if (sub < NX // 2) == (way == 0):
                    receive()
                else:
                    pl.when(step < far)(receive)

    def maybe_attend(plane, extra=True):
        @pl.when((plane < z) & extra)
        def _():
            attend(plane, False)

    @pl.loop(1, far + 1)
    def _(step):
        kv_step(step)

        @pl.when(step == far)
        def _():
            for dy in range(1, n_tp):
                place = wo_all.at[wrap(tp - dy, n_tp), :, :, c]
                remote(
                    place, place, oy_send.at[dy - 1], oy_recv.at[dy - 1], z, x, c, tp
                ).wait_recv()
                wo_twin(n_tp - dy, c).start()

        maybe_attend(plane_at(1, step - 1), step > 1)
        twin_step(step)
        maybe_attend(plane_at(0, step))

    my_head = tp * NX + x
    quarter = rows // 2
    low_lane = lax.broadcasted_iota(jnp.int32, (quarter, LANES), 1) < HEAD_DIM

    def att_copy(rel, dy):
        i, yy = wrap(x + rel, NX), wrap(tp + dy, n_tp)
        return remote(
            att_send.at[i, yy], att_recv.at[my_head], at_send.at[rel, dy],
            at_recv.at[my_head], z, i, c, yy,
        )

    for rel in (2, 1, 3, 0):
        i = wrap(x + rel, NX)
        acc = run_acc[i]
        att = acc[:HEAD_DIM] / acc[HEAD_DIM : HEAD_DIM + 1]
        att = jnp.concatenate([att, att], axis=0).T
        for y in range(n_tp):
            first = att[y * rows : y * rows + quarter]
            second = att[y * rows + quarter : (y + 1) * rows]
            att_send[i, y] = jnp.where(low_lane, first, second).astype(BF16)
        for dy in (2, 1, 3, 0):
            if rel or dy:
                att_copy(rel, dy).start()
    att_recv[my_head] = att_send[x, tp]

    for dy in range(n_tp):
        wo_twin(dy, other).wait_recv()
    for k in range(1, NX * n_tp):
        source = wrap(my_head + k, NX * n_tp)
        place = att_recv.at[source]
        remote(place, place, at_send.at[0, 0], at_recv.at[source], z, x, c, tp).wait_recv()

    projected = jnp.zeros((rows, model), F32)
    for y in range(n_tp):
        pieces = []
        for pair in range(NX // 2):
            even = att_recv[y * NX + 2 * pair].astype(F32)
            odd = att_recv[y * NX + 2 * pair + 1].astype(F32)
            first = jnp.where(low_lane, even, pltpu.roll(odd, HEAD_DIM, axis=1))
            second = jnp.where(low_lane, pltpu.roll(even, HEAD_DIM, axis=1), odd)
            pieces.append(jnp.concatenate([first, second], axis=0).astype(BF16))
        columns = jnp.concatenate(pieces, axis=1)
        projected = projected + lax.dot_general(
            columns, wo_all[y].reshape(model, width), CONTRACT_LAST, preferred_element_type=F32
        )
    out_ref[...] = rms_norm(projected, out_gain_ref[...])

    for d in range(1, NX):
        forget_x(d).wait_send()
        wo_x(d).wait_send()
        gate_x(d).wait_send()
        kv_x(d).wait_send()
        q_x(d).wait_send()
    for d in range(1, n_tp):
        tok_copy(d).wait_send()
        wo_y(d).wait_send()
    for d in range(n_tp):
        wo_twin(d, c).wait_send()
    forget_twin(c).wait_send()
    for k in range(1, nz):
        forget_z(k).wait_send()
        wo_z(k).wait_send()
    for a in (0, 1):
        @pl.loop(0, nz)
        def _(k):
            for dx in range(NX):
                if dx > 0:
                    w_x(a, k, dx).wait_send()
                w_twin(a, k, dx, c).wait_send()

        for k in range(1, nz):
            w_z(a, k).wait_send()
    for k in range(1, nz * NC):
        gate_z(k).wait_send()
    for step in range(0, far + 1):
        for way in both:
            if step == 0 and way == 1:
                continue
            for sub in range(NX) if step == 0 else ring_subs(way, step):
                twin(kv_all, kd_send, kd_recv, way, step, sub, c).wait_send()
                if step > 0:
                    ring_hop(kv_all, kz_send, kz_recv, way, step, sub).wait_send()
    for rel in range(NX):
        for dy in range(n_tp):
            if rel or dy:
                att_copy(rel, dy).wait_send()


def solution(mesh):
    n_sp, n_tp = mesh.shape["sp"], mesh.shape["tp"]
    nz = n_sp // (NX * NC)

    def on_device(
        tokens, norm_gain, w_query, w_key, w_value, w_forget, forget_offset, w_out_t, out_gain
    ):
        rows, model = tokens.shape
        w_rows, width = w_query.shape
        heads = w_forget.shape[1]
        block = rows * n_tp
        half = block // 2
        far = nz // 2
        vmem = pl.BlockSpec(memory_space=pltpu.VMEM)
        anywhere = pl.BlockSpec(memory_space=pl.ANY)
        dma = pltpu.SemaphoreType.DMA

        def pair(*shape):
            return [dma(shape), dma(shape)]

        return pl.pallas_call(
            functools.partial(layer_kernel, nz, n_tp),
            out_shape=jax.ShapeDtypeStruct((rows, model), BF16),
            in_specs=[
                vmem, vmem, anywhere, anywhere, anywhere, vmem,
                pl.BlockSpec(memory_space=pltpu.SMEM), anywhere, vmem,
            ],
            out_specs=vmem,
            scratch_shapes=[
                pltpu.VMEM((n_tp, rows, model), BF16),
                pltpu.VMEM((nz, NX, NC, w_rows, 2 * width), BF16),
                pltpu.VMEM((nz, NX, NC, w_rows, width), BF16),
                pltpu.VMEM((n_tp, nz, NX, NC, w_rows, width), BF16),
                pltpu.VMEM((nz, NX, NC, 8, w_rows), F32),
                pltpu.VMEM((heads, 1, block), F32),
                pltpu.VMEM((nz, NX, NC, 1, block), F32),
                pltpu.VMEM((nz, LANES, LANES), BF16),
                pltpu.VMEM((heads, block, LANES), BF16),
                pltpu.VMEM((nz, NX, NC, block, LANES), BF16),
                pltpu.VMEM((heads, HEAD_DIM, block), BF16),
                pltpu.VMEM((NX, HEAD_DIM, block), BF16),
                pltpu.VMEM((NX, 2, block, block), BF16),
                pltpu.VMEM((NX * NC * half, 2 * LANES), BF16),
                pltpu.VMEM((NX, 2, NX * NC * half, block), F32),
                pltpu.VMEM((NX, 1, block), F32),
                pltpu.VMEM((NX, HEAD_DIM + 16, block), F32),
                pltpu.VMEM((NX, n_tp, rows // 2, LANES), BF16),
                pltpu.VMEM((NX * n_tp, rows // 2, LANES), BF16),
                dma((4,)),
                *pair(n_tp - 1),
                *pair(2, nz),
                *pair(2, nz, NX),
                *pair(2, nz, NX),
                *pair(nz - 1),
                *pair(NX - 1),
                *pair(1),
                *pair(nz - 1),
                *pair(NX - 1),
                *pair(n_tp - 1),
                *pair(n_tp),
                *pair(NX - 1),
                *pair(nz * NC - 1),
                *pair(NX - 1),
                *pair(NX - 1),
                *pair(2, far, NX),
                *pair(2, far + 1, NX),
                dma((NX, n_tp)),
                dma((NX * n_tp,)),
            ],
            compiler_params=pltpu.CompilerParams(collective_id=0, has_side_effects=True),
        )(
            tokens, norm_gain.reshape(1, model), w_query, w_key, w_value, w_forget.T,
            forget_offset, w_out_t, out_gain.reshape(1, model),
        )

    return jax.shard_map(
        on_device,
        mesh=mesh,
        in_specs=(
            P(("sp", "tp"), None),
            P(),
            P("sp", "tp"),
            P("sp", "tp"),
            P("sp", "tp"),
            P("sp", "tp"),
            P("tp"),
            P("sp", "tp"),
            P(),
        ),
        out_specs=P(("sp", "tp"), None),
        check_vma=False,
    )
```

time: 76.1 us -> 72.3 us (0.950)
  the two profiles are of different devices: /device:TPU:224 before, /device:TPU:1 now
where the time goes in v2:
time: 72.3 us; the launch traced here: 72.1 us
  Pallas kernels  70.6 us (98%)
  local copies, waits for them, and re-layouts  1.57 us (2%)
    pallas_call x1, Pallas kernels, on_device(): pl.pallas_call(functools.partial(layer_kernel, nz, n_tp), out_shape=jax.S...  70.6 us
    unnamed x1, local copies, waits for them, and re-layouts  1.57 us

profile of v2, /device:TPU:1, one launch (start us, length us, event | category | flops | bytes accessed | tf_op | source)
XLA Modules:
  0.0 72.1 jit_solution(2916909153270804277)
XLA Ops:
  0.0 70.6 %shard_map.91 = bf16[64,1024]{1,0:T(8,128)(2,1)} custom-call(bf16[64,1024]{1,0:T(8,128)(2,1)} %tokens_ref.1, f32[1,1024]{1,0:T(1,128)} %bitcast.3, bf16[16,256]{1,0:T(8,128)(2,1)} %wq_ref.1, bf16[16,256]{1,0:T(8,128)(2,1)} %wk_ref.1, bf16[16,256]{1,0:T(8,128)(2,1)} %wv_ref.1, bf16[4,16]{1,0:T(4,128)(2,1)} %bitcast.5, f32[4]{0:T(128)} %offset_ref.1, ...), custom_call_target="tpu_custom_call" | custom-call | tf_op jit(solution)/shard_map/pallas_call | solution.py:658
  70.6 1.6 %copy.11 = bf16[64,1024]{1,0:T(8,128)(2,1)} copy(bf16[64,1024]{1,0:T(8,128)(2,1)} %shard_map.91) | data formatting | bytes 262144

commit v3 on v2

--- a/solution.py
+++ b/solution.py
@@ -11,7 +11,7 @@
 LANES = 128
 NORM_EPS = 1e-06
 NX, NC = 4, 2
-CHUNK, LAG = 4, 4
+CHUNK, LAG = 2, 8
 MESH = pl.DeviceIdType.MESH
 F32 = jnp.float32
 BF16 = jnp.bfloat16
@@ -28,7 +28,7 @@
     tokens_ref, gain_ref, wq_ref, wk_ref, wv_ref, wf_ref, offset_ref, wo_ref, out_gain_ref,
     out_ref,
     normed, w_kv, w_q, wo_all, forget_all, gates_send, gates_all, bias_all,
-    kv_send, kv_all, q_send, q_recv, q_rhs, left, scores, run_max, run_acc, att_send, att_recv,
+    kv_send, kv_all, q_send, q_recv, q_rhs, key_side, scores, run_max, run_acc, att_send, att_recv,
     local_sem, tok_send, tok_recv, wz_send, wz_recv, wx_send, wx_recv, wd_send, wd_recv,
     fz_send, fz_recv, fx_send, fx_recv, fd_send, fd_recv,
     oz_send, oz_recv, ox_send, ox_recv, oy_send, oy_recv, od_send, od_recv,
@@ -60,6 +60,12 @@
             device_id=(at(zz, xx, cc), yy), device_id_type=MESH,
         )
 
+    def landed(view, sem):
+        remote(view, view, sem, sem, z, x, 1 - c, tp).wait_recv()
+
+    def left(view, sem):
+        remote(view, view, sem, sem, z, x, 1 - c, tp).wait_send()
+
     up, down = wrap(z + 1, nz), wrap(z - 1, nz)
     other = 1 - c
 
@@ -98,59 +104,43 @@
     def w_z(a, k):
         place = w_place(a, 0, 0, c)
         return remote(
-            place, place, wz_send.at[a, k], wz_recv.at[a, k], wrap(z + k, nz), x, c, tp
+            place, place, wz_send.at[a], wz_recv.at[a, k], wrap(z + k, nz), x, c, tp
         )
 
     def w_x(a, k, dx):
         place = w_place(a, k, 0, c)
         return remote(
-            place, place, wx_send.at[a, k, dx], wx_recv.at[a, k, dx],
+            place, place, wx_send.at[a], wx_recv.at[a, k],
             z, wrap(x + dx, NX), c, tp,
         )
 
-    def w_twin(a, k, dx, core):
-        place = w_place(a, k, dx, core)
-        return remote(
-            place, place, wd_send.at[a, k, dx], wd_recv.at[a, k, dx], z, x, other, tp
-        )
+    def w_twin(a, k):
+        place = weights[a].at[wrap(z - k, nz), :, c]
+        return remote(place, place, wd_send.at[a], wd_recv.at[a], z, x, other, tp)
 
     def w_onward(a, k):
         for dx in (2, 1, 3):
             w_x(a, k, dx).start()
-        w_twin(a, k, 0, c).start()
 
     def nearest(n):
         return jnp.where(lax.rem(n, 2) == 1, lax.div(n + 1, 2), nz - lax.div(n, 2))
 
-    def w_from_z(a):
-        w_onward(a, 0)
-
-        @pl.loop(1, nz)
+    def w_from_z(a, first, last):
+        @pl.loop(first, last)
         def _(n):
             k = nearest(n)
-            place = w_place(a, k, 0, c)
-            remote(
-                place, place, wz_send.at[a, k], wz_recv.at[a, k], up, x, c, tp
-            ).wait_recv()
+            landed(w_place(a, k, 0, c), wz_recv.at[a, k])
             w_onward(a, k)
 
     def w_from_x(a):
         @pl.loop(0, nz)
         def _(n):
             k = jnp.where(n == 0, 0, nearest(n))
-            for dx in (1, 3, 2):
-                place = w_place(a, k, NX - dx, c)
-                remote(
-                    place, place, wx_send.at[a, k, dx], wx_recv.at[a, k, dx],
-                    z, wrap(x + 1, NX), c, tp,
-                ).wait_recv()
-                w_twin(a, k, NX - dx, c).start()
+            landed(weights[a].at[0, pl.ds(0, NX - 1), c], wx_recv.at[a, k])
+            w_twin(a, k).start()
 
     def w_from_twin(a):
-        @pl.loop(0, nz)
-        def _(k):
-            for dx in range(NX):
-                w_twin(a, k, dx, other).wait_recv()
+        landed(weights[a].at[:, :, other], wd_recv.at[a])
 
     def ring_subs(way, step):
         if step < far:
@@ -163,39 +153,35 @@
     def ring_hop(ref, send, recv, way, step, sub):
         place = ref.at[plane_at(way, step - 1), wrap(x + sub, NX), c]
         return remote(
-            place, place, send.at[way, step - 1, sub], recv.at[way, step - 1, sub],
+            place, place, send.at[way], recv.at[way, step - 1, sub],
             (up, down)[way], x, c, tp,
         )
 
     def ring_wait(ref, send, recv, way, step, sub):
+        landed(
+            ref.at[plane_at(way, step), wrap(x + sub, NX), c], recv.at[way, step - 1, sub]
+        )
+
+    def twin(ref, send, recv, way, step, sub):
         place = ref.at[plane_at(way, step), wrap(x + sub, NX), c]
-        remote(
-            place, place, send.at[way, step - 1, sub], recv.at[way, step - 1, sub],
-            (up, down)[way], x, c, tp,
-        ).wait_recv()
-
-    def twin(ref, send, recv, way, step, sub, core):
-        place = ref.at[plane_at(way, step), wrap(x + sub, NX), core]
-        return remote(
-            place, place, send.at[way, step, sub], recv.at[way, step, sub], z, x, other, tp
-        )
+        return remote(place, place, send.at[0], recv.at[way, step], z, x, other, tp)
 
     def tok_copy(dy):
         return remote(
-            normed.at[tp], normed.at[tp], tok_send.at[dy - 1], tok_recv.at[dy - 1],
+            normed.at[tp], normed.at[tp], tok_send.at[0], tok_recv.at[0],
             z, x, c, wrap(tp + dy, n_tp),
         )
 
     def forget_z(k):
         place = forget_all.at[z, x, c]
         return remote(
-            place, place, fz_send.at[k - 1], fz_recv.at[k - 1], wrap(z + k, nz), x, c, tp
+            place, place, fz_send.at[0], fz_recv.at[0], wrap(z + k, nz), x, c, tp
         )
 
     def forget_x(dx):
         place = forget_all.at[:, x, c]
         return remote(
-            place, place, fx_send.at[dx - 1], fx_recv.at[dx - 1], z, wrap(x + dx, NX), c, tp
+            place, place, fx_send.at[0], fx_recv.at[0], z, wrap(x + dx, NX), c, tp
         )
 
     def forget_twin(core):
@@ -205,57 +191,50 @@
     def wo_z(k):
         place = wo_all.at[tp, z, x, c]
         return remote(
-            place, place, oz_send.at[k - 1], oz_recv.at[k - 1], wrap(z + k, nz), x, c, tp
+            place, place, oz_send.at[0], oz_recv.at[0], wrap(z + k, nz), x, c, tp
         )
 
     def wo_x(dx):
         place = wo_all.at[tp, :, x, c]
         return remote(
-            place, place, ox_send.at[dx - 1], ox_recv.at[dx - 1], z, wrap(x + dx, NX), c, tp
+            place, place, ox_send.at[0], ox_recv.at[0], z, wrap(x + dx, NX), c, tp
         )
 
     def wo_y(dy):
         place = wo_all.at[tp, :, :, c]
         return remote(
-            place, place, oy_send.at[dy - 1], oy_recv.at[dy - 1], z, x, c, wrap(tp + dy, n_tp)
-        )
-
-    def wo_twin(dy, core):
-        place = wo_all.at[wrap(tp + dy, n_tp), :, :, core]
-        return remote(place, place, od_send.at[dy], od_recv.at[dy], z, x, other, tp)
+            place, place, oy_send.at[0], oy_recv.at[0], z, x, c, wrap(tp + dy, n_tp)
+        )
+
+    def wo_twin(dy):
+        place = wo_all.at[wrap(tp + dy, n_tp), :, :, c]
+        return remote(place, place, od_send.at[0], od_recv.at[0], z, x, other, tp)
 
     both = (0, 1)
     far_first = sorted(range(1, nz), key=lambda k: -min(k, nz - k))
+    for k in far_first:
+        forget_z(k).start()
     for k in far_first:
         w_z(0, k).start()
     for dy in range(1, n_tp):
         tok_copy(dy).start()
     for k in far_first:
-        forget_z(k).start()
-    for k in far_first:
         w_z(1, k).start()
     for k in far_first:
         wo_z(k).start()
 
-    w_from_z(0)
-    for k in range(1, nz):
-        place = forget_all.at[wrap(z - k, nz), x, c]
-        remote(place, place, fz_send.at[k - 1], fz_recv.at[k - 1], up, x, c, tp).wait_recv()
+    w_onward(0, 0)
+    w_from_z(0, 1, 5)
+    landed(forget_all.at[pl.ds(0, nz - 1), 0, 0], fz_recv.at[0])
     for dx in range(1, NX):
         forget_x(dx).start()
-    w_from_z(1)
+    w_from_z(0, 5, nz)
+    w_onward(1, 0)
+    w_from_z(1, 1, nz)
     w_from_x(0)
-    for dx in range(1, NX):
-        place = forget_all.at[:, wrap(x - dx, NX), c]
-        remote(
-            place, place, fx_send.at[dx - 1], fx_recv.at[dx - 1], z, x, c, tp
-        ).wait_recv()
+    landed(forget_all.at[:, pl.ds(0, NX - 1), 0], fx_recv.at[0])
     forget_twin(c).start()
-    for dy in range(1, n_tp):
-        place = normed.at[wrap(tp - dy, n_tp)]
-        remote(
-            place, place, tok_send.at[dy - 1], tok_recv.at[dy - 1], z, x, c, tp
-        ).wait_recv()
+    landed(normed.at[pl.ds(0, n_tp - 1)], tok_recv.at[0])
     tokens_here = normed[...].reshape(block, model)
     forget_twin(other).wait_recv()
     forget_rows = jnp.concatenate(
@@ -288,7 +267,7 @@
     def gate_x(dx):
         hx = wrap(x + dx, NX)
         return remote(
-            gates_send.at[hx], gates_all.at[z, x, c], gx_send.at[dx - 1], gx_recv.at[dx - 1],
+            gates_send.at[hx], gates_all.at[z, x, c], gx_send.at[0], gx_recv.at[0],
             z, hx, c, tp,
         )
 
@@ -319,7 +298,7 @@
     def kv_x(dx):
         hx = wrap(x + dx, NX)
         return remote(
-            kv_send.at[hx], kv_all.at[z, x, c], kx_send.at[dx - 1], kx_recv.at[dx - 1],
+            kv_send.at[hx], kv_all.at[z, x, c], kx_send.at[0], kx_recv.at[dx - 1],
             z, hx, c, tp,
         )
 
@@ -328,27 +307,34 @@
     kv_all[z, x, c] = kv_send[x]
     for way in both:
         ring_hop(kv_all, kz_send, kz_recv, way, 1, 0).start()
-    twin(kv_all, kd_send, kd_recv, 0, 0, 0, c).start()
-
-    for dx in range(1, NX):
-        place = gates_all.at[z, wrap(x - dx, NX), c]
-        remote(
-            place, place, gx_send.at[dx - 1], gx_recv.at[dx - 1], z, x, c, tp
-        ).wait_recv()
+    twin(kv_all, kd_send, kd_recv, 0, 0, 0).start()
+
+    landed(gates_all.at[0, pl.ds(0, NX - 1), 0], gx_recv.at[0])
 
     def gate_z(k):
         cc = c if k % NC == 0 else other
         place = gates_all.at[z, :, c]
-        return remote(
-            place, place, gz_send.at[k - 1], gz_recv.at[k - 1],
+        group = min(k - 1, 1)
+        return remote(
+            place, place, gz_send.at[group], gz_recv.at[group],
             wrap(z + k // NC, nz), x, cc, tp,
         )
 
     for k in range(1, nz * NC):
         gate_z(k).start()
 
+    def first_sub(step):
+        for way in both:
+            if 0 not in ring_subs(way, step):
+                continue
+            ring_wait(kv_all, kz_send, kz_recv, way, step, 0)
+            if step < far and 0 in ring_subs(way, step + 1):
+                ring_hop(kv_all, kz_send, kz_recv, way, step + 1, 0).start()
+            twin(kv_all, kd_send, kd_recv, way, step, 0).start()
+
     w_from_x(1)
     w_from_twin(1)
+    first_sub(1)
     queries_t = (project(w_q, 0).astype(BF16).astype(F32) * HEAD_DIM ** (-0.5)).T.astype(BF16)
     for h in range(heads):
         q_send[h] = queries_t[h * HEAD_DIM : (h + 1) * HEAD_DIM]
@@ -356,32 +342,23 @@
     def q_x(dx):
         hx = wrap(x + dx, NX)
         return remote(
-            q_send.at[hx], q_recv.at[x], qx_send.at[dx - 1], qx_recv.at[dx - 1], z, hx, c, tp
+            q_send.at[hx], q_recv.at[x], qx_send.at[0], qx_recv.at[0], z, hx, c, tp
         )
 
     for dx in range(1, NX):
         q_x(dx).start()
     q_recv[x] = q_send[x]
 
-    for sub in range(1, NX):
+    first_sub(2)
+    for sub in (1, 3, 2):
         dx = NX - sub
-        place = kv_all.at[z, wrap(x + sub, NX), c]
-        remote(
-            place, place, kx_send.at[dx - 1], kx_recv.at[dx - 1], z, x, c, tp
-        ).wait_recv()
+        landed(kv_all.at[z, wrap(x + sub, NX), c], kx_recv.at[dx - 1])
         for way in both:
             ring_hop(kv_all, kz_send, kz_recv, way, 1, sub).start()
-        twin(kv_all, kd_send, kd_recv, 0, 0, sub, c).start()
-
-    for dx in range(1, NX):
-        place = q_recv.at[wrap(x - dx, NX)]
-        remote(
-            place, place, qx_send.at[dx - 1], qx_recv.at[dx - 1], z, x, c, tp
-        ).wait_recv()
-
-    for k in range(1, nz):
-        place = wo_all.at[tp, wrap(z - k, nz), x, c]
-        remote(place, place, oz_send.at[k - 1], oz_recv.at[k - 1], up, x, c, tp).wait_recv()
+        twin(kv_all, kd_send, kd_recv, 0, 0, sub).start()
+
+    landed(q_recv.at[pl.ds(0, NX - 1)], qx_recv.at[0])
+    landed(wo_all.at[0, pl.ds(0, nz - 1), 0, 0], oz_recv.at[0])
     for dx in range(1, NX):
         wo_x(dx).start()
     ones_at = lax.broadcasted_iota(jnp.int32, (LANES, block), 0)
@@ -393,12 +370,9 @@
             parts = [q_recv[i], no_rows] if side == 0 else [no_rows, q_recv[i]]
             q_rhs[i, side] = jnp.concatenate(parts + [picks], axis=0)
 
-    for k in range(1, nz * NC):
-        cc = c if k % NC == 0 else other
-        place = gates_all.at[wrap(z - k // NC, nz), :, cc]
-        remote(
-            place, place, gz_send.at[k - 1], gz_recv.at[k - 1], z, x, other, tp
-        ).wait_recv()
+    first_sub(3)
+    landed(gates_all.at[0, :, 0], gz_recv.at[0])
+    landed(gates_all.at[pl.ds(0, nz - 1), :, :], gz_recv.at[1])
 
     n_blocks = nz * plane_blocks
     gate_rows = gates_all[...].reshape(n_blocks, block)
@@ -435,11 +409,11 @@
             jnp.where(lane_block == b, 1.0, 0.0)[:1].astype(BF16) for b in range(plane_blocks)
         ]
         bias_tiles = jnp.concatenate([bias_cols * mask for mask in masks], axis=0)
-        left[...] = jnp.concatenate([key_rows, bias_tiles], axis=1)
+        key_side[...] = jnp.concatenate([key_rows, bias_tiles], axis=1)
 
         def score(i, side, b0):
             span = slice(b0 * half, (b0 + CHUNK) * half)
-            s = jnp.dot(left[span, :], q_rhs[i, side], preferred_element_type=F32)
+            s = jnp.dot(key_side[span, :], q_rhs[i, side], preferred_element_type=F32)
             if own:
                 row = lax.broadcasted_iota(jnp.int32, s.shape, 0)
                 key_at = (b0 + row // half) * block + side * half + row % half
@@ -473,7 +447,7 @@
 
         chunks = [
             (i, side, b0)
-            for i in range(NX) for side in (0, 1) for b0 in range(0, plane_blocks, CHUNK)
+            for side in (0, 1) for b0 in range(0, plane_blocks, CHUNK) for i in range(NX)
         ]
         tops = []
         for n in range(len(chunks) + LAG):
@@ -482,27 +456,23 @@
             if n >= LAG:
                 absorb(*chunks[n - LAG], tops[n - LAG])
 
-    for sub in range(NX):
-        twin(kv_all, kd_send, kd_recv, 0, 0, sub, other).wait_recv()
+    landed(kv_all.at[z, :, other], kd_recv.at[0, 0])
     attend(z, True)
 
-    for dx in range(1, NX):
-        place = wo_all.at[tp, :, wrap(x - dx, NX), c]
-        remote(
-            place, place, ox_send.at[dx - 1], ox_recv.at[dx - 1], z, x, c, tp
-        ).wait_recv()
+    landed(wo_all.at[tp, :, pl.ds(0, NX - 1), c], ox_recv.at[0])
     for dy in range(1, n_tp):
         wo_y(dy).start()
-    wo_twin(0, c).start()
-
-    def kv_step(step):
-        for sub in range(NX):
+    wo_twin(0).start()
+    first_sub(4)
+
+    def kv_step(step, subs):
+        for sub in subs:
             for way in both:
                 whole = (sub < NX // 2) == (way == 0)
 
                 def receive():
                     ring_wait(kv_all, kz_send, kz_recv, way, step, sub)
-                    twin(kv_all, kd_send, kd_recv, way, step, sub, c).start()
+                    twin(kv_all, kd_send, kd_recv, way, step, sub).start()
 
                     @pl.when(step + (0 if whole else 1) < far)
                     def _():
@@ -514,16 +484,18 @@
                     pl.when(step < far)(receive)
 
     def twin_step(step):
-        for sub in range(NX):
-            for way in both:
-
-                def receive():
-                    twin(kv_all, kd_send, kd_recv, way, step, sub, other).wait_recv()
-
-                if (sub < NX // 2) == (way == 0):
-                    receive()
-                else:
-                    pl.when(step < far)(receive)
+        for way in both:
+
+            @pl.when(step < far)
+            def _():
+                landed(kv_all.at[plane_at(way, step), :, other], kd_recv.at[way, step])
+
+            @pl.when(step == far)
+            def _():
+                landed(
+                    kv_all.at[plane_at(way, step), pl.ds(0, NX // 2), other],
+                    kd_recv.at[way, step],
+                )
 
     def maybe_attend(plane, extra=True):
         @pl.when((plane < z) & extra)
@@ -532,18 +504,16 @@
 
     @pl.loop(1, far + 1)
     def _(step):
-        kv_step(step)
+        kv_step(step, (1,))
+        maybe_attend(plane_at(1, step - 1), step > 1)
+        kv_step(step, (2, 3))
 
         @pl.when(step == far)
         def _():
+            landed(wo_all.at[pl.ds(0, n_tp - 1), :, :, c], oy_recv.at[0])
             for dy in range(1, n_tp):
-                place = wo_all.at[wrap(tp - dy, n_tp), :, :, c]
-                remote(
-                    place, place, oy_send.at[dy - 1], oy_recv.at[dy - 1], z, x, c, tp
-                ).wait_recv()
-                wo_twin(n_tp - dy, c).start()
-
-        maybe_attend(plane_at(1, step - 1), step > 1)
+                wo_twin(dy).start()
+
         twin_step(step)
         maybe_attend(plane_at(0, step))
 
@@ -554,8 +524,8 @@
     def att_copy(rel, dy):
         i, yy = wrap(x + rel, NX), wrap(tp + dy, n_tp)
         return remote(
-            att_send.at[i, yy], att_recv.at[my_head], at_send.at[rel, dy],
-            at_recv.at[my_head], z, i, c, yy,
+            att_send.at[i, yy], att_recv.at[my_head], at_send.at[0],
+            at_recv.at[0], z, i, c, yy,
         )
 
     for rel in (2, 1, 3, 0):
@@ -572,12 +542,8 @@
                 att_copy(rel, dy).start()
     att_recv[my_head] = att_send[x, tp]
 
-    for dy in range(n_tp):
-        wo_twin(dy, other).wait_recv()
-    for k in range(1, NX * n_tp):
-        source = wrap(my_head + k, NX * n_tp)
-        place = att_recv.at[source]
-        remote(place, place, at_send.at[0, 0], at_recv.at[source], z, x, c, tp).wait_recv()
+    landed(wo_all.at[:, :, :, other], od_recv.at[0])
+    landed(att_recv.at[pl.ds(0, NX * n_tp - 1)], at_recv.at[0])
 
     projected = jnp.zeros((rows, model), F32)
     for y in range(n_tp):
@@ -594,45 +560,27 @@
         )
     out_ref[...] = rms_norm(projected, out_gain_ref[...])
 
-    for d in range(1, NX):
-        forget_x(d).wait_send()
-        wo_x(d).wait_send()
-        gate_x(d).wait_send()
-        kv_x(d).wait_send()
-        q_x(d).wait_send()
-    for d in range(1, n_tp):
-        tok_copy(d).wait_send()
-        wo_y(d).wait_send()
-    for d in range(n_tp):
-        wo_twin(d, c).wait_send()
+    for a in (0, 1):
+        left(weights[a].at[pl.ds(0, nz - 1), 0, 0], wz_send.at[a])
+        left(weights[a].at[:, pl.ds(0, NX - 1), 0], wx_send.at[a])
+        left(weights[a].at[:, :, c], wd_send.at[a])
+    left(normed.at[pl.ds(0, n_tp - 1)], tok_send.at[0])
+    left(forget_all.at[pl.ds(0, nz - 1), 0, 0], fz_send.at[0])
+    left(forget_all.at[:, pl.ds(0, NX - 1), 0], fx_send.at[0])
     forget_twin(c).wait_send()
-    for k in range(1, nz):
-        forget_z(k).wait_send()
-        wo_z(k).wait_send()
-    for a in (0, 1):
-        @pl.loop(0, nz)
-        def _(k):
-            for dx in range(NX):
-                if dx > 0:
-                    w_x(a, k, dx).wait_send()
-                w_twin(a, k, dx, c).wait_send()
-
-        for k in range(1, nz):
-            w_z(a, k).wait_send()
-    for k in range(1, nz * NC):
-        gate_z(k).wait_send()
-    for step in range(0, far + 1):
-        for way in both:
-            if step == 0 and way == 1:
-                continue
-            for sub in range(NX) if step == 0 else ring_subs(way, step):
-                twin(kv_all, kd_send, kd_recv, way, step, sub, c).wait_send()
-                if step > 0:
-                    ring_hop(kv_all, kz_send, kz_recv, way, step, sub).wait_send()
-    for rel in range(NX):
-        for dy in range(n_tp):
-            if rel or dy:
-                att_copy(rel, dy).wait_send()
+    left(wo_all.at[0, pl.ds(0, nz - 1), 0, 0], oz_send.at[0])
+    left(wo_all.at[0, :, pl.ds(0, NX - 1), 0], ox_send.at[0])
+    left(wo_all.at[pl.ds(0, n_tp - 1), :, :, 0], oy_send.at[0])
+    left(wo_all.at[:, :, :, 0], od_send.at[0])
+    left(gates_all.at[0, pl.ds(0, NX - 1), 0], gx_send.at[0])
+    left(gates_all.at[0, :, 0], gz_send.at[0])
+    left(gates_all.at[pl.ds(0, nz - 1), :, :], gz_send.at[1])
+    left(kv_send.at[pl.ds(0, NX - 1)], kx_send.at[0])
+    left(q_send.at[pl.ds(0, NX - 1)], qx_send.at[0])
+    left(kv_all.at[:, :, 0], kd_send.at[0])
+    for way in both:
+        left(kv_all.at[pl.ds(0, nz - 1), pl.ds(0, NX // 2), 0], kz_send.at[way])
+    left(att_recv.at[pl.ds(0, NX * n_tp - 1)], at_send.at[0])
 
 
 def solution(mesh):
@@ -684,25 +632,24 @@
                 pltpu.VMEM((NX, n_tp, rows // 2, LANES), BF16),
                 pltpu.VMEM((NX * n_tp, rows // 2, LANES), BF16),
                 dma((4,)),
-                *pair(n_tp - 1),
-                *pair(2, nz),
-                *pair(2, nz, NX),
-                *pair(2, nz, NX),
-                *pair(nz - 1),
-                *pair(NX - 1),
-                *pair(1),
-                *pair(nz - 1),
-                *pair(NX - 1),
-                *pair(n_tp - 1),
-                *pair(n_tp),
-                *pair(NX - 1),
-                *pair(nz * NC - 1),
-                *pair(NX - 1),
-                *pair(NX - 1),
-                *pair(2, far, NX),
-                *pair(2, far + 1, NX),
-                dma((NX, n_tp)),
-                dma((NX * n_tp,)),
+                *pair(1),
+                dma((2,)), dma((2, nz)),
+                dma((2,)), dma((2, nz)),
+                *pair(2),
+                *pair(1),
+                *pair(1),
+                *pair(1),
+                *pair(1),
+                *pair(1),
+                *pair(1),
+                *pair(1),
+                *pair(1),
+                *pair(2),
+                dma((1,)), dma((NX - 1,)),
+                *pair(1),
+                dma((2,)), dma((2, far, NX)),
+                dma((1,)), dma((2, far + 1)),
+                *pair(1),
             ],
             compiler_params=pltpu.CompilerParams(collective_id=0, has_side_effects=True),
         )(

time: 72.3 us -> 68.8 us (0.952)
  the two profiles are of different devices: /device:TPU:1 before, /device:TPU:224 now
where the time goes in v3:
time: 68.8 us; the launch traced here: 68.5 us
  Pallas kernels  67 us (97%)
  local copies, waits for them, and re-layouts  1.57 us (2%)
    pallas_call x1, Pallas kernels, on_device(): pl.pallas_call(functools.partial(layer_kernel, nz, n_tp), out_shape=jax.S...  67 us
    unnamed x1, local copies, waits for them, and re-layouts  1.57 us

profile of v3, /device:TPU:224, one launch (start us, length us, event | category | flops | bytes accessed | tf_op | source)
XLA Modules:
  0.0 68.5 jit_solution(7984203398299489231)
XLA Ops:
  0.0 67.0 %shard_map.91 = bf16[64,1024]{1,0:T(8,128)(2,1)} custom-call(bf16[64,1024]{1,0:T(8,128)(2,1)} %tokens_ref.1, f32[1,1024]{1,0:T(1,128)} %bitcast.3, bf16[16,256]{1,0:T(8,128)(2,1)} %wq_ref.1, bf16[16,256]{1,0:T(8,128)(2,1)} %wk_ref.1, bf16[16,256]{1,0:T(8,128)(2,1)} %wv_ref.1, bf16[4,16]{1,0:T(4,128)(2,1)} %bitcast.5, f32[4]{0:T(128)} %offset_ref.1, ...), custom_call_target="tpu_custom_call" | custom-call | tf_op jit(solution)/shard_map/pallas_call | solution.py:606
  67.0 1.6 %copy.11 = bf16[64,1024]{1,0:T(8,128)(2,1)} copy(bf16[64,1024]{1,0:T(8,128)(2,1)} %shard_map.91) | data formatting | bytes 262144

commit v4 on v3

--- a/solution.py
+++ b/solution.py
@@ -90,8 +90,9 @@
     for device in near:
         pl.semaphore_signal(barrier, inc=1, device_id_type=MESH, device_id=device)
 
+    w_rows = wf_ref.shape[1]
     forget_all[z, x, c] = jnp.concatenate(
-        [wf_ref[...].astype(F32), jnp.zeros((8 - heads, wf_ref.shape[1]), F32)], axis=0
+        [wf_ref[...].astype(F32), jnp.zeros((heads, LANES - w_rows), F32)], axis=1
     )
     normed[tp] = rms_norm(tokens_ref[...].astype(F32), gain_ref[...])
     for copy in local:
@@ -117,6 +118,12 @@
     def w_twin(a, k):
         place = weights[a].at[wrap(z - k, nz), :, c]
         return remote(place, place, wd_send.at[a], wd_recv.at[a], z, x, other, tp)
+
+    def w_group_z(k):
+        place = w_q.at[z, :, c]
+        return remote(
+            place, place, wz_send.at[1], wz_recv.at[1, k], wrap(z + k, nz), x, c, tp
+        )
 
     def w_onward(a, k):
         for dx in (2, 1, 3):
@@ -132,12 +139,12 @@
             landed(w_place(a, k, 0, c), wz_recv.at[a, k])
             w_onward(a, k)
 
-    def w_from_x(a):
-        @pl.loop(0, nz)
+    def w_from_x(first, last):
+        @pl.loop(first, last)
         def _(n):
             k = jnp.where(n == 0, 0, nearest(n))
-            landed(weights[a].at[0, pl.ds(0, NX - 1), c], wx_recv.at[a, k])
-            w_twin(a, k).start()
+            landed(w_kv.at[0, pl.ds(0, NX - 1), c], wx_recv.at[0, k])
+            w_twin(0, k).start()
 
     def w_from_twin(a):
         landed(weights[a].at[:, :, other], wd_recv.at[a])
@@ -216,33 +223,40 @@
         forget_z(k).start()
     for k in far_first:
         w_z(0, k).start()
+    for dx in (2, 1, 3):
+        w_x(1, 0, dx).start()
     for dy in range(1, n_tp):
         tok_copy(dy).start()
+
+    w_onward(0, 0)
+    w_from_z(0, 1, 3)
+    landed(w_q.at[0, pl.ds(0, NX - 1), c], wx_recv.at[1, 0])
     for k in far_first:
-        w_z(1, k).start()
+        w_group_z(k).start()
     for k in far_first:
         wo_z(k).start()
-
-    w_onward(0, 0)
-    w_from_z(0, 1, 5)
+    w_twin(1, 0).start()
+    w_from_z(0, 3, 5)
     landed(forget_all.at[pl.ds(0, nz - 1), 0, 0], fz_recv.at[0])
     for dx in range(1, NX):
         forget_x(dx).start()
     w_from_z(0, 5, nz)
-    w_onward(1, 0)
-    w_from_z(1, 1, nz)
-    w_from_x(0)
+    w_from_x(0, 5)
     landed(forget_all.at[:, pl.ds(0, NX - 1), 0], fx_recv.at[0])
     forget_twin(c).start()
+    w_from_x(5, nz)
     landed(normed.at[pl.ds(0, n_tp - 1)], tok_recv.at[0])
     tokens_here = normed[...].reshape(block, model)
     forget_twin(other).wait_recv()
     forget_rows = jnp.concatenate(
         [
-            forget_all[i // plane_blocks, (i // NC) % NX, i % NC]
+            forget_all[i // plane_blocks, (i // NC) % NX, i % NC][:, :w_rows]
             for i in range(nz * plane_blocks)
         ],
         axis=1,
+    )
+    forget_rows = jnp.concatenate(
+        [forget_rows, jnp.zeros((8 - heads, model), F32)], axis=0
     ).astype(BF16)
     logits = lax.dot_general(
         forget_rows, tokens_here, CONTRACT_LAST, preferred_element_type=F32
@@ -309,20 +323,6 @@
         ring_hop(kv_all, kz_send, kz_recv, way, 1, 0).start()
     twin(kv_all, kd_send, kd_recv, 0, 0, 0).start()
 
-    landed(gates_all.at[0, pl.ds(0, NX - 1), 0], gx_recv.at[0])
-
-    def gate_z(k):
-        cc = c if k % NC == 0 else other
-        place = gates_all.at[z, :, c]
-        group = min(k - 1, 1)
-        return remote(
-            place, place, gz_send.at[group], gz_recv.at[group],
-            wrap(z + k // NC, nz), x, cc, tp,
-        )
-
-    for k in range(1, nz * NC):
-        gate_z(k).start()
-
     def first_sub(step):
         for way in both:
             if 0 not in ring_subs(way, step):
@@ -332,9 +332,13 @@
                 ring_hop(kv_all, kz_send, kz_recv, way, step + 1, 0).start()
             twin(kv_all, kd_send, kd_recv, way, step, 0).start()
 
-    w_from_x(1)
+    @pl.loop(1, nz)
+    def _(n):
+        k = nearest(n)
+        landed(w_q.at[0, :, c], wz_recv.at[1, k])
+        w_twin(1, k).start()
+
     w_from_twin(1)
-    first_sub(1)
     queries_t = (project(w_q, 0).astype(BF16).astype(F32) * HEAD_DIM ** (-0.5)).T.astype(BF16)
     for h in range(heads):
         q_send[h] = queries_t[h * HEAD_DIM : (h + 1) * HEAD_DIM]
@@ -349,7 +353,21 @@
         q_x(dx).start()
     q_recv[x] = q_send[x]
 
-    first_sub(2)
+    landed(gates_all.at[0, pl.ds(0, NX - 1), 0], gx_recv.at[0])
+
+    def gate_z(k):
+        cc = c if k % NC == 0 else other
+        place = gates_all.at[z, :, c]
+        group = min(k - 1, 1)
+        return remote(
+            place, place, gz_send.at[group], gz_recv.at[group],
+            wrap(z + k // NC, nz), x, cc, tp,
+        )
+
+    for k in range(1, nz * NC):
+        gate_z(k).start()
+
+    first_sub(1)
     for sub in (1, 3, 2):
         dx = NX - sub
         landed(kv_all.at[z, wrap(x + sub, NX), c], kx_recv.at[dx - 1])
@@ -370,7 +388,6 @@
             parts = [q_recv[i], no_rows] if side == 0 else [no_rows, q_recv[i]]
             q_rhs[i, side] = jnp.concatenate(parts + [picks], axis=0)
 
-    first_sub(3)
     landed(gates_all.at[0, :, 0], gz_recv.at[0])
     landed(gates_all.at[pl.ds(0, nz - 1), :, :], gz_recv.at[1])
 
@@ -402,19 +419,26 @@
     lane_block = lax.broadcasted_iota(jnp.int32, (8, LANES), 1) % 8
     ones_rows = jnp.ones((16, CHUNK * half), BF16)
 
-    def attend(plane, own):
-        key_rows = kv_all[plane, :, :, :half, :].reshape(plane_blocks * half, LANES)
+    def attend(plane, own, core=None):
+        if core is None:
+            blocks = [(b // NC, b % NC) for b in range(plane_blocks)]
+            key_rows = kv_all[plane, :, :, :half, :].reshape(plane_blocks * half, LANES)
+        else:
+            blocks = [(b, core) for b in range(NX)]
+            key_rows = kv_all[plane, :, core, :half, :].reshape(NX * half, LANES)
+        lag = LAG if core is None else LAG // 2
         bias_cols = bias_all[plane]
         masks = [
-            jnp.where(lane_block == b, 1.0, 0.0)[:1].astype(BF16) for b in range(plane_blocks)
+            jnp.where(lane_block == xx * NC + cc, 1.0, 0.0)[:1].astype(BF16)
+            for xx, cc in blocks
         ]
         bias_tiles = jnp.concatenate([bias_cols * mask for mask in masks], axis=0)
-        key_side[...] = jnp.concatenate([key_rows, bias_tiles], axis=1)
+        key_side[: len(blocks) * half, :] = jnp.concatenate([key_rows, bias_tiles], axis=1)
 
         def score(i, side, b0):
             span = slice(b0 * half, (b0 + CHUNK) * half)
             s = jnp.dot(key_side[span, :], q_rhs[i, side], preferred_element_type=F32)
-            if own:
+            if own and b0 == i * NC:
                 row = lax.broadcasted_iota(jnp.int32, s.shape, 0)
                 key_at = (b0 + row // half) * block + side * half + row % half
                 query_at = lax.broadcasted_iota(jnp.int32, s.shape, 1) + (
@@ -437,8 +461,8 @@
             lo = half + side * HEAD_DIM
             value_cols = jnp.concatenate(
                 [
-                    kv_all[plane, b // NC, b % NC, lo : lo + HEAD_DIM, :]
-                    for b in range(b0, b0 + CHUNK)
+                    kv_all[plane, xx, cc, lo : lo + HEAD_DIM, :]
+                    for xx, cc in blocks[b0 : b0 + CHUNK]
                 ],
                 axis=1,
             )
@@ -447,23 +471,25 @@
 
         chunks = [
             (i, side, b0)
-            for side in (0, 1) for b0 in range(0, plane_blocks, CHUNK) for i in range(NX)
+            for side in (0, 1) for b0 in range(0, len(blocks), CHUNK) for i in range(NX)
+            if not own or b0 <= i * NC
         ]
         tops = []
-        for n in range(len(chunks) + LAG):
+        for n in range(len(chunks) + lag):
             if n < len(chunks):
                 tops.append(score(*chunks[n]))
-            if n >= LAG:
-                absorb(*chunks[n - LAG], tops[n - LAG])
+            if n >= lag:
+                absorb(*chunks[n - lag], tops[n - lag])
 
     landed(kv_all.at[z, :, other], kd_recv.at[0, 0])
     attend(z, True)
-
-    landed(wo_all.at[tp, :, pl.ds(0, NX - 1), c], ox_recv.at[0])
-    for dy in range(1, n_tp):
-        wo_y(dy).start()
-    wo_twin(0).start()
-    first_sub(4)
+    first_sub(2)
+
+    def wo_along_y():
+        landed(wo_all.at[tp, :, pl.ds(0, NX - 1), c], ox_recv.at[0])
+        for dy in range(1, n_tp):
+            wo_y(dy).start()
+        wo_twin(0).start()
 
     def kv_step(step, subs):
         for sub in subs:
@@ -497,14 +523,17 @@
                     kd_recv.at[way, step],
                 )
 
-    def maybe_attend(plane, extra=True):
+    def maybe_attend(plane, extra, core=None):
         @pl.when((plane < z) & extra)
         def _():
-            attend(plane, False)
+            attend(plane, False, core)
 
     @pl.loop(1, far + 1)
     def _(step):
         kv_step(step, (1,))
+        pl.when(step == 1)(wo_along_y)
+        pl.when(step == 2)(lambda: first_sub(3))
+        pl.when(step == 3)(lambda: first_sub(4))
         maybe_attend(plane_at(1, step - 1), step > 1)
         kv_step(step, (2, 3))
 
@@ -514,8 +543,11 @@
             for dy in range(1, n_tp):
                 wo_twin(dy).start()
 
-        twin_step(step)
-        maybe_attend(plane_at(0, step))
+        @pl.loop(0, NC)
+        def _(part):
+            pl.when(part == 1)(lambda: twin_step(step))
+            maybe_attend(plane_at(0, step), True, lax.rem(c + part, NC))
+
 
     my_head = tp * NX + x
     quarter = rows // 2
@@ -560,9 +592,11 @@
         )
     out_ref[...] = rms_norm(projected, out_gain_ref[...])
 
+    left(w_kv.at[pl.ds(0, nz - 1), 0, 0], wz_send.at[0])
+    left(w_kv.at[:, pl.ds(0, NX - 1), 0], wx_send.at[0])
+    left(w_q.at[pl.ds(0, nz - 1), :, 0], wz_send.at[1])
+    left(w_q.at[0, pl.ds(0, NX - 1), 0], wx_send.at[1])
     for a in (0, 1):
-        left(weights[a].at[pl.ds(0, nz - 1), 0, 0], wz_send.at[a])
-        left(weights[a].at[:, pl.ds(0, NX - 1), 0], wx_send.at[a])
         left(weights[a].at[:, :, c], wd_send.at[a])
     left(normed.at[pl.ds(0, n_tp - 1)], tok_send.at[0])
     left(forget_all.at[pl.ds(0, nz - 1), 0, 0], fz_send.at[0])
@@ -616,7 +650,7 @@
                 pltpu.VMEM((nz, NX, NC, w_rows, 2 * width), BF16),
                 pltpu.VMEM((nz, NX, NC, w_rows, width), BF16),
                 pltpu.VMEM((n_tp, nz, NX, NC, w_rows, width), BF16),
-                pltpu.VMEM((nz, NX, NC, 8, w_rows), F32),
+                pltpu.VMEM((nz, NX, NC, heads, LANES), F32),
                 pltpu.VMEM((heads, 1, block), F32),
                 pltpu.VMEM((nz, NX, NC, 1, block), F32),
                 pltpu.VMEM((nz, LANES, LANES), BF16),

time: 68.8 us -> 61.5 us (0.89)
  Pallas kernels: 67 us -> 59.3 us
    pallas_call x1, Pallas kernels: 67 us -> 59.3 us  [on_device(): pl.pallas_call(functools.partial(layer_kernel, nz, n_tp), out_shape=jax.S...]
where the time goes in v4:
time: 61.5 us; the launch traced here: 60.9 us
  Pallas kernels  59.3 us (96%)
  local copies, waits for them, and re-layouts  1.57 us (3%)
    pallas_call x1, Pallas kernels, on_device(): pl.pallas_call(functools.partial(layer_kernel, nz, n_tp), out_shape=jax.S...  59.3 us
    unnamed x1, local copies, waits for them, and re-layouts  1.57 us

profile of v4, /device:TPU:224, one launch (start us, length us, event | category | flops | bytes accessed | tf_op | source)
XLA Modules:
  0.0 60.9 jit_solution(15205594450392065091)
XLA Ops:
  0.0 59.3 %shard_map.91 = bf16[64,1024]{1,0:T(8,128)(2,1)} custom-call(bf16[64,1024]{1,0:T(8,128)(2,1)} %tokens_ref.1, f32[1,1024]{1,0:T(1,128)} %bitcast.3, bf16[16,256]{1,0:T(8,128)(2,1)} %wq_ref.1, bf16[16,256]{1,0:T(8,128)(2,1)} %wk_ref.1, bf16[16,256]{1,0:T(8,128)(2,1)} %wv_ref.1, bf16[4,16]{1,0:T(4,128)(2,1)} %bitcast.5, f32[4]{0:T(128)} %offset_ref.1, ...), custom_call_target="tpu_custom_call" | custom-call | tf_op jit(solution)/shard_map/pallas_call | solution.py:640
  59.3 1.6 %copy.11 = bf16[64,1024]{1,0:T(8,128)(2,1)} copy(bf16[64,1024]{1,0:T(8,128)(2,1)} %shard_map.91) | data formatting | bytes 262144

commit v5 on v4

--- a/solution.py
+++ b/solution.py
@@ -11,7 +11,7 @@
 LANES = 128
 NORM_EPS = 1e-06
 NX, NC = 4, 2
-CHUNK, LAG = 2, 8
+WHOLE, HALVES = (1, 16), (2, 8)
 MESH = pl.DeviceIdType.MESH
 F32 = jnp.float32
 BF16 = jnp.bfloat16
@@ -28,12 +28,12 @@
     tokens_ref, gain_ref, wq_ref, wk_ref, wv_ref, wf_ref, offset_ref, wo_ref, out_gain_ref,
     out_ref,
     normed, w_kv, w_q, wo_all, forget_all, gates_send, gates_all, bias_all,
-    kv_send, kv_all, q_send, q_recv, q_rhs, key_side, scores, run_max, run_acc, att_send, att_recv,
+    kv_send, kv_relay, kv_all, q_send, q_recv, q_rhs, key_side, scores, run_max, run_acc, att_send, att_recv,
     local_sem, tok_send, tok_recv, wz_send, wz_recv, wx_send, wx_recv, wd_send, wd_recv,
     fz_send, fz_recv, fx_send, fx_recv, fd_send, fd_recv,
     oz_send, oz_recv, ox_send, ox_recv, oy_send, oy_recv, od_send, od_recv,
     gx_send, gx_recv, gz_send, gz_recv, kx_send, kx_recv, qx_send, qx_recv,
-    kz_send, kz_recv, kd_send, kd_recv, at_send, at_recv,
+    kz_send, kz_recv, kr_send, kr_recv, kt_send, kd_send, kd_recv, at_send, at_recv,
 ):
     sp, tp = lax.axis_index("sp"), lax.axis_index("tp")
     z = lax.div(sp, NX * NC)
@@ -160,7 +160,7 @@
     def ring_hop(ref, send, recv, way, step, sub):
         place = ref.at[plane_at(way, step - 1), wrap(x + sub, NX), c]
         return remote(
-            place, place, send.at[way], recv.at[way, step - 1, sub],
+            place, place, send.at[way, min(sub, 1)], recv.at[way, step - 1, sub],
             (up, down)[way], x, c, tp,
         )
 
@@ -316,12 +316,28 @@
             z, hx, c, tp,
         )
 
-    for dx in range(1, NX):
+    for dx in (2, 1, 3):
         kv_x(dx).start()
     kv_all[z, x, c] = kv_send[x]
     for way in both:
         ring_hop(kv_all, kz_send, kz_recv, way, 1, 0).start()
     twin(kv_all, kd_send, kd_recv, 0, 0, 0).start()
+
+    def kv_off(way, dx):
+        return remote(
+            kv_send.at[wrap(x + dx, NX)], kv_relay.at[way, dx - 1],
+            kr_send.at[0], kr_recv.at[way, dx - 1], (up, down)[way], x, c, tp,
+        )
+
+    def kv_turn(way, dx):
+        return remote(
+            kv_relay.at[way, dx - 1], kv_all.at[plane_at(way, 1), x, c],
+            kt_send.at[0], kz_recv.at[way, 0, NX - dx], z, wrap(x + dx, NX), c, tp,
+        )
+
+    for dx in (2, 1, 3):
+        for way in both:
+            kv_off(way, dx).start()
 
     def first_sub(step):
         for way in both:
@@ -368,12 +384,12 @@
         gate_z(k).start()
 
     first_sub(1)
-    for sub in (1, 3, 2):
-        dx = NX - sub
-        landed(kv_all.at[z, wrap(x + sub, NX), c], kx_recv.at[dx - 1])
+    for dx in (2, 1, 3):
         for way in both:
-            ring_hop(kv_all, kz_send, kz_recv, way, 1, sub).start()
-        twin(kv_all, kd_send, kd_recv, 0, 0, sub).start()
+            landed(kv_relay.at[way, dx - 1], kr_recv.at[way, dx - 1])
+            kv_turn(way, dx).start()
+        landed(kv_all.at[z, wrap(x - dx, NX), c], kx_recv.at[dx - 1])
+        twin(kv_all, kd_send, kd_recv, 0, 0, NX - dx).start()
 
     landed(q_recv.at[pl.ds(0, NX - 1)], qx_recv.at[0])
     landed(wo_all.at[0, pl.ds(0, nz - 1), 0, 0], oz_recv.at[0])
@@ -417,7 +433,6 @@
         bias_all[zz] = jnp.concatenate(stack + [no_bias], axis=0).T.astype(BF16)
 
     lane_block = lax.broadcasted_iota(jnp.int32, (8, LANES), 1) % 8
-    ones_rows = jnp.ones((16, CHUNK * half), BF16)
 
     def attend(plane, own, core=None):
         if core is None:
@@ -426,7 +441,7 @@
         else:
             blocks = [(b, core) for b in range(NX)]
             key_rows = kv_all[plane, :, core, :half, :].reshape(NX * half, LANES)
-        lag = LAG if core is None else LAG // 2
+        size, lag = WHOLE if core is None else HALVES
         bias_cols = bias_all[plane]
         masks = [
             jnp.where(lane_block == xx * NC + cc, 1.0, 0.0)[:1].astype(BF16)
@@ -436,9 +451,9 @@
         key_side[: len(blocks) * half, :] = jnp.concatenate([key_rows, bias_tiles], axis=1)
 
         def score(i, side, b0):
-            span = slice(b0 * half, (b0 + CHUNK) * half)
+            span = slice(b0 * half, (b0 + size) * half)
             s = jnp.dot(key_side[span, :], q_rhs[i, side], preferred_element_type=F32)
-            if own and b0 == i * NC:
+            if own and b0 + size > i * NC:
                 row = lax.broadcasted_iota(jnp.int32, s.shape, 0)
                 key_at = (b0 + row // half) * block + side * half + row % half
                 query_at = lax.broadcasted_iota(jnp.int32, s.shape, 1) + (
@@ -456,23 +471,25 @@
                 top = jnp.maximum(old, top)
                 total = run_acc[i] * jnp.exp(old - top)
             run_max[i] = top
-            span = slice(b0 * half, (b0 + CHUNK) * half)
+            span = slice(b0 * half, (b0 + size) * half)
             weights = jnp.exp(scores[i, side, span, :] - top).astype(BF16)
             lo = half + side * HEAD_DIM
             value_cols = jnp.concatenate(
                 [
                     kv_all[plane, xx, cc, lo : lo + HEAD_DIM, :]
-                    for xx, cc in blocks[b0 : b0 + CHUNK]
+                    for xx, cc in blocks[b0 : b0 + size]
                 ],
                 axis=1,
             )
-            value_cols = jnp.concatenate([value_cols, ones_rows], axis=0)
+            value_cols = jnp.concatenate(
+                [value_cols, jnp.ones((16, size * half), BF16)], axis=0
+            )
             run_acc[i] = total + jnp.dot(value_cols, weights, preferred_element_type=F32)
 
         chunks = [
             (i, side, b0)
-            for side in (0, 1) for b0 in range(0, len(blocks), CHUNK) for i in range(NX)
-            if not own or b0 <= i * NC
+            for side in (0, 1) for b0 in range(0, len(blocks), size) for i in range(NX)
+            if not own or b0 < (i + 1) * NC
         ]
         tops = []
         for n in range(len(chunks) + lag):
@@ -531,23 +548,21 @@
     @pl.loop(1, far + 1)
     def _(step):
         kv_step(step, (1,))
-        pl.when(step == 1)(wo_along_y)
         pl.when(step == 2)(lambda: first_sub(3))
+        pl.when(step == 2)(wo_along_y)
         pl.when(step == 3)(lambda: first_sub(4))
         maybe_attend(plane_at(1, step - 1), step > 1)
         kv_step(step, (2, 3))
-
-        @pl.when(step == far)
-        def _():
-            landed(wo_all.at[pl.ds(0, n_tp - 1), :, :, c], oy_recv.at[0])
-            for dy in range(1, n_tp):
-                wo_twin(dy).start()
 
         @pl.loop(0, NC)
         def _(part):
             pl.when(part == 1)(lambda: twin_step(step))
             maybe_attend(plane_at(0, step), True, lax.rem(c + part, NC))
 
+
+    landed(wo_all.at[pl.ds(0, n_tp - 1), :, :, c], oy_recv.at[0])
+    for dy in range(1, n_tp):
+        wo_twin(dy).start()
 
     my_head = tp * NX + x
     quarter = rows // 2
@@ -612,8 +627,15 @@
     left(kv_send.at[pl.ds(0, NX - 1)], kx_send.at[0])
     left(q_send.at[pl.ds(0, NX - 1)], qx_send.at[0])
     left(kv_all.at[:, :, 0], kd_send.at[0])
+    left(kv_all.at[pl.ds(0, 2 * (NX - 1)), 0, 0], kr_send.at[0])
+    left(kv_all.at[pl.ds(0, 2 * (NX - 1)), 0, 0], kt_send.at[0])
     for way in both:
-        left(kv_all.at[pl.ds(0, nz - 1), pl.ds(0, NX // 2), 0], kz_send.at[way])
+        for early in (0, 1):
+            count = sum(
+                (sub == 0) == (early == 0) and (sub == 0 or step > 1)
+                for step in range(1, far + 1) for sub in ring_subs(way, step)
+            )
+            left(kv_all.at[pl.ds(0, count), 0, 0], kz_send.at[way, early])
     left(att_recv.at[pl.ds(0, NX * n_tp - 1)], at_send.at[0])
 
 
@@ -655,6 +677,7 @@
                 pltpu.VMEM((nz, NX, NC, 1, block), F32),
                 pltpu.VMEM((nz, LANES, LANES), BF16),
                 pltpu.VMEM((heads, block, LANES), BF16),
+                pltpu.VMEM((2, NX - 1, block, LANES), BF16),
                 pltpu.VMEM((nz, NX, NC, block, LANES), BF16),
                 pltpu.VMEM((heads, HEAD_DIM, block), BF16),
                 pltpu.VMEM((NX, HEAD_DIM, block), BF16),
@@ -681,7 +704,8 @@
                 *pair(2),
                 dma((1,)), dma((NX - 1,)),
                 *pair(1),
-                dma((2,)), dma((2, far, NX)),
+                dma((2, 2)), dma((2, far, NX)),
+                dma((1,)), dma((2, NX - 1)), dma((1,)),
                 dma((1,)), dma((2, far + 1)),
                 *pair(1),
             ],

time: 61.5 us -> 64.8 us (1.054)
  Pallas kernels: 59.3 us -> 62.6 us
    pallas_call x1, Pallas kernels: 59.3 us -> 62.6 us  [on_device(): pl.pallas_call(functools.partial(layer_kernel, nz, n_tp), out_shape=jax.S...]
where the time goes in v5:
time: 64.8 us; the launch traced here: 64.2 us
  Pallas kernels  62.6 us (97%)
  local copies, waits for them, and re-layouts  1.57 us (2%)
    pallas_call x1, Pallas kernels, on_device(): pl.pallas_call(functools.partial(layer_kernel, nz, n_tp), out_shape=jax.S...  62.6 us
    unnamed x1, local copies, waits for them, and re-layouts  1.57 us

profile of v5, /device:TPU:224, one launch (start us, length us, event | category | flops | bytes accessed | tf_op | source)
XLA Modules:
  0.0 64.2 jit_solution(10161721363218943505)
XLA Ops:
  0.0 62.6 %shard_map.91 = bf16[64,1024]{1,0:T(8,128)(2,1)} custom-call(bf16[64,1024]{1,0:T(8,128)(2,1)} %tokens_ref.1, f32[1,1024]{1,0:T(1,128)} %bitcast.3, bf16[16,256]{1,0:T(8,128)(2,1)} %wq_ref.1, bf16[16,256]{1,0:T(8,128)(2,1)} %wk_ref.1, bf16[16,256]{1,0:T(8,128)(2,1)} %wv_ref.1, bf16[4,16]{1,0:T(4,128)(2,1)} %bitcast.5, f32[4]{0:T(128)} %offset_ref.1, ...), custom_call_target="tpu_custom_call" | custom-call | tf_op jit(solution)/shard_map/pallas_call | solution.py:662
  62.6 1.6 %copy.11 = bf16[64,1024]{1,0:T(8,128)(2,1)} copy(bf16[64,1024]{1,0:T(8,128)(2,1)} %shard_map.91) | data formatting | bytes 262144

commit v6 on v4

--- a/solution.py
+++ b/solution.py
@@ -426,7 +426,6 @@
         else:
             blocks = [(b, core) for b in range(NX)]
             key_rows = kv_all[plane, :, core, :half, :].reshape(NX * half, LANES)
-        lag = LAG if core is None else LAG // 2
         bias_cols = bias_all[plane]
         masks = [
             jnp.where(lane_block == xx * NC + cc, 1.0, 0.0)[:1].astype(BF16)
@@ -475,11 +474,11 @@
             if not own or b0 <= i * NC
         ]
         tops = []
-        for n in range(len(chunks) + lag):
+        for n in range(len(chunks) + LAG):
             if n < len(chunks):
                 tops.append(score(*chunks[n]))
-            if n >= lag:
-                absorb(*chunks[n - lag], tops[n - lag])
+            if n >= LAG:
+                absorb(*chunks[n - LAG], tops[n - LAG])
 
     landed(kv_all.at[z, :, other], kd_recv.at[0, 0])
     attend(z, True)
@@ -531,17 +530,11 @@
     @pl.loop(1, far + 1)
     def _(step):
         kv_step(step, (1,))
-        pl.when(step == 1)(wo_along_y)
         pl.when(step == 2)(lambda: first_sub(3))
+        pl.when(step == 2)(wo_along_y)
         pl.when(step == 3)(lambda: first_sub(4))
         maybe_attend(plane_at(1, step - 1), step > 1)
         kv_step(step, (2, 3))
-
-        @pl.when(step == far)
-        def _():
-            landed(wo_all.at[pl.ds(0, n_tp - 1), :, :, c], oy_recv.at[0])
-            for dy in range(1, n_tp):
-                wo_twin(dy).start()
 
         @pl.loop(0, NC)
         def _(part):
@@ -573,6 +566,9 @@
             if rel or dy:
                 att_copy(rel, dy).start()
     att_recv[my_head] = att_send[x, tp]
+    landed(wo_all.at[pl.ds(0, n_tp - 1), :, :, c], oy_recv.at[0])
+    for dy in range(1, n_tp):
+        wo_twin(dy).start()
 
     landed(wo_all.at[:, :, :, other], od_recv.at[0])
     landed(att_recv.at[pl.ds(0, NX * n_tp - 1)], at_recv.at[0])

time: 61.5 us -> 61.5 us (level)
  the two profiles are of different devices: /device:TPU:224 before, /device:TPU:1 now
where the time goes in v6:
time: 61.5 us; the launch traced here: 61.3 us
  Pallas kernels  59.7 us (97%)
  local copies, waits for them, and re-layouts  1.57 us (3%)
    pallas_call x1, Pallas kernels, on_device(): pl.pallas_call(functools.partial(layer_kernel, nz, n_tp), out_shape=jax.S...  59.7 us
    unnamed x1, local copies, waits for them, and re-layouts  1.57 us

profile of v6, /device:TPU:1, one launch (start us, length us, event | category | flops | bytes accessed | tf_op | source)
XLA Modules:
  0.0 61.3 jit_solution(11519871378362692519)
XLA Ops:
  0.0 59.7 %shard_map.91 = bf16[64,1024]{1,0:T(8,128)(2,1)} custom-call(bf16[64,1024]{1,0:T(8,128)(2,1)} %tokens_ref.1, f32[1,1024]{1,0:T(1,128)} %bitcast.3, bf16[16,256]{1,0:T(8,128)(2,1)} %wq_ref.1, bf16[16,256]{1,0:T(8,128)(2,1)} %wk_ref.1, bf16[16,256]{1,0:T(8,128)(2,1)} %wv_ref.1, bf16[4,16]{1,0:T(4,128)(2,1)} %bitcast.5, f32[4]{0:T(128)} %offset_ref.1, ...), custom_call_target="tpu_custom_call" | custom-call | tf_op jit(solution)/shard_map/pallas_call | solution.py:636
  59.7 1.6 %copy.11 = bf16[64,1024]{1,0:T(8,128)(2,1)} copy(bf16[64,1024]{1,0:T(8,128)(2,1)} %shard_map.91) | data formatting | bytes 262144

commit v7 on v6

--- a/solution.py
+++ b/solution.py
@@ -149,18 +149,31 @@
     def w_from_twin(a):
         landed(weights[a].at[:, :, other], wd_recv.at[a])
 
-    def ring_subs(way, step):
-        if step < far:
-            return (0, 1, 2, 3)
-        return (0, 1) if way == 0 else (2, 3)
-
     def plane_at(way, step):
         return wrap(z - step, nz) if way == 0 else wrap(z + step, nz)
 
+    def steps_of(way, sub):
+        return far if (sub < NX // 2) == (way == 0) else far - 1
+
+    def sends(way, step, sub):
+        inside = step <= steps_of(way, sub)
+        if way == 0:
+            return inside & (z >= step - 1) & (z < nz - 1)
+        return inside & (wrap(z + step - 1, nz) < steps_of(way, sub))
+
+    def receives(way, step, sub):
+        inside = step <= steps_of(way, sub)
+        if way == 0:
+            return inside & (z >= step)
+        return inside & (wrap(z + step, nz) < steps_of(way, sub))
+
+    def reads(way, step):
+        return z >= step if way == 0 else z + step >= nz
+
     def ring_hop(ref, send, recv, way, step, sub):
         place = ref.at[plane_at(way, step - 1), wrap(x + sub, NX), c]
         return remote(
-            place, place, send.at[way], recv.at[way, step - 1, sub],
+            place, place, send.at[way, step - 1, sub], recv.at[way, step - 1, sub],
             (up, down)[way], x, c, tp,
         )
 
@@ -171,7 +184,7 @@
 
     def twin(ref, send, recv, way, step, sub):
         place = ref.at[plane_at(way, step), wrap(x + sub, NX), c]
-        return remote(place, place, send.at[0], recv.at[way, step], z, x, other, tp)
+        return remote(place, place, send.at[way, step], recv.at[way, step], z, x, other, tp)
 
     def tok_copy(dy):
         return remote(
@@ -319,18 +332,32 @@
     for dx in range(1, NX):
         kv_x(dx).start()
     kv_all[z, x, c] = kv_send[x]
-    for way in both:
-        ring_hop(kv_all, kz_send, kz_recv, way, 1, 0).start()
-    twin(kv_all, kd_send, kd_recv, 0, 0, 0).start()
+
+    def ring_enter(sub):
+        for way in both:
+            pl.when(sends(way, 1, sub))(
+                lambda way=way: ring_hop(kv_all, kz_send, kz_recv, way, 1, sub).start()
+            )
+        twin(kv_all, kd_send, kd_recv, 0, 0, sub).start()
+
+    ring_enter(0)
+
+    def ring_poll(way, step, sub):
+        @pl.when(receives(way, step, sub))
+        def _():
+            ring_wait(kv_all, kz_send, kz_recv, way, step, sub)
+
+            @pl.when(sends(way, step + 1, sub))
+            def _():
+                ring_hop(kv_all, kz_send, kz_recv, way, step + 1, sub).start()
+
+            @pl.when(reads(way, step))
+            def _():
+                twin(kv_all, kd_send, kd_recv, way, step, sub).start()
 
     def first_sub(step):
         for way in both:
-            if 0 not in ring_subs(way, step):
-                continue
-            ring_wait(kv_all, kz_send, kz_recv, way, step, 0)
-            if step < far and 0 in ring_subs(way, step + 1):
-                ring_hop(kv_all, kz_send, kz_recv, way, step + 1, 0).start()
-            twin(kv_all, kd_send, kd_recv, way, step, 0).start()
+            ring_poll(way, step, 0)
 
     @pl.loop(1, nz)
     def _(n):
@@ -371,9 +398,7 @@
     for sub in (1, 3, 2):
         dx = NX - sub
         landed(kv_all.at[z, wrap(x + sub, NX), c], kx_recv.at[dx - 1])
-        for way in both:
-            ring_hop(kv_all, kz_send, kz_recv, way, 1, sub).start()
-        twin(kv_all, kd_send, kd_recv, 0, 0, sub).start()
+        ring_enter(sub)
 
     landed(q_recv.at[pl.ds(0, NX - 1)], qx_recv.at[0])
     landed(wo_all.at[0, pl.ds(0, nz - 1), 0, 0], oz_recv.at[0])
@@ -493,29 +518,16 @@
     def kv_step(step, subs):
         for sub in subs:
             for way in both:
-                whole = (sub < NX // 2) == (way == 0)
-
-                def receive():
-                    ring_wait(kv_all, kz_send, kz_recv, way, step, sub)
-                    twin(kv_all, kd_send, kd_recv, way, step, sub).start()
-
-                    @pl.when(step + (0 if whole else 1) < far)
-                    def _():
-                        ring_hop(kv_all, kz_send, kz_recv, way, step + 1, sub).start()
-
-                if whole:
-                    receive()
-                else:
-                    pl.when(step < far)(receive)
+                ring_poll(way, step, sub)
 
     def twin_step(step):
         for way in both:
 
-            @pl.when(step < far)
+            @pl.when(reads(way, step) & (step < far))
             def _():
                 landed(kv_all.at[plane_at(way, step), :, other], kd_recv.at[way, step])
 
-            @pl.when(step == far)
+            @pl.when(reads(way, step) & (step == far))
             def _():
                 landed(
                     kv_all.at[plane_at(way, step), pl.ds(0, NX // 2), other],
@@ -607,9 +619,21 @@
     left(gates_all.at[pl.ds(0, nz - 1), :, :], gz_send.at[1])
     left(kv_send.at[pl.ds(0, NX - 1)], kx_send.at[0])
     left(q_send.at[pl.ds(0, NX - 1)], qx_send.at[0])
-    left(kv_all.at[:, :, 0], kd_send.at[0])
+    left(kv_all.at[0, :, 0], kd_send.at[0, 0])
     for way in both:
-        left(kv_all.at[pl.ds(0, nz - 1), pl.ds(0, NX // 2), 0], kz_send.at[way])
+        for step in range(1, far + 1):
+            count = NX if step < far else NX // 2
+
+            @pl.when(reads(way, step))
+            def _():
+                left(kv_all.at[0, pl.ds(0, count), 0], kd_send.at[way, step])
+
+            for sub in range(NX):
+                if step <= steps_of(way, sub):
+
+                    @pl.when(sends(way, step, sub))
+                    def _():
+                        left(kv_all.at[0, 0, 0], kz_send.at[way, step - 1, sub])
     left(att_recv.at[pl.ds(0, NX * n_tp - 1)], at_send.at[0])
 
 
@@ -677,8 +701,8 @@
                 *pair(2),
                 dma((1,)), dma((NX - 1,)),
                 *pair(1),
-                dma((2,)), dma((2, far, NX)),
-                dma((1,)), dma((2, far + 1)),
+                *pair(2, far, NX),
+                *pair(2, far + 1),
                 *pair(1),
             ],
             compiler_params=pltpu.CompilerParams(collective_id=0, has_side_effects=True),

time: 61.5 us -> 60.4 us (0.982)
  the two profiles are of different devices: /device:TPU:1 before, /device:TPU:224 now
where the time goes in v7:
time: 60.4 us; the launch traced here: 59.9 us
  Pallas kernels  58.4 us (97%)
  local copies, waits for them, and re-layouts  1.57 us (3%)
    pallas_call x1, Pallas kernels, on_device(): pl.pallas_call(functools.partial(layer_kernel, nz, n_tp), out_shape=jax.S...  58.4 us
    unnamed x1, local copies, waits for them, and re-layouts  1.57 us

profile of v7, /device:TPU:224, one launch (start us, length us, event | category | flops | bytes accessed | tf_op | source)
XLA Modules:
  0.0 59.9 jit_solution(11744406924183162086)
XLA Ops:
  0.0 58.4 %shard_map.91 = bf16[64,1024]{1,0:T(8,128)(2,1)} custom-call(bf16[64,1024]{1,0:T(8,128)(2,1)} %tokens_ref.1, f32[1,1024]{1,0:T(1,128)} %bitcast.3, bf16[16,256]{1,0:T(8,128)(2,1)} %wq_ref.1, bf16[16,256]{1,0:T(8,128)(2,1)} %wk_ref.1, bf16[16,256]{1,0:T(8,128)(2,1)} %wv_ref.1, bf16[4,16]{1,0:T(4,128)(2,1)} %bitcast.5, f32[4]{0:T(128)} %offset_ref.1, ...), custom_call_target="tpu_custom_call" | custom-call | tf_op jit(solution)/shard_map/pallas_call | solution.py:660
  58.4 1.6 %copy.11 = bf16[64,1024]{1,0:T(8,128)(2,1)} copy(bf16[64,1024]{1,0:T(8,128)(2,1)} %shard_map.91) | data formatting | bytes 262144

commit v8 on v7

--- a/solution.py
+++ b/solution.py
@@ -539,18 +539,24 @@
         def _():
             attend(plane, False, core)
 
+    kv_step(1, (1,))
+
     @pl.loop(1, far + 1)
     def _(step):
-        kv_step(step, (1,))
+        kv_step(step, (2,))
         pl.when(step == 2)(lambda: first_sub(3))
-        pl.when(step == 2)(wo_along_y)
         pl.when(step == 3)(lambda: first_sub(4))
         maybe_attend(plane_at(1, step - 1), step > 1)
-        kv_step(step, (2, 3))
+        kv_step(step, (3,))
+        pl.when(step == 1)(wo_along_y)
 
         @pl.loop(0, NC)
         def _(part):
-            pl.when(part == 1)(lambda: twin_step(step))
+            @pl.when(part == 1)
+            def _():
+                twin_step(step)
+                kv_step(step + 1, (1,))
+
             maybe_attend(plane_at(0, step), True, lax.rem(c + part, NC))
 
 

time: 60.4 us -> 61.3 us (1.015)
  Pallas kernels: 58.4 us -> 59.2 us
    pallas_call x1, Pallas kernels: 58.4 us -> 59.2 us  [on_device(): pl.pallas_call(functools.partial(layer_kernel, nz, n_tp), out_shape=jax.S...]
where the time goes in v8:
time: 61.3 us; the launch traced here: 60.8 us
  Pallas kernels  59.2 us (97%)
  local copies, waits for them, and re-layouts  1.57 us (3%)
    pallas_call x1, Pallas kernels, on_device(): pl.pallas_call(functools.partial(layer_kernel, nz, n_tp), out_shape=jax.S...  59.2 us
    unnamed x1, local copies, waits for them, and re-layouts  1.57 us

profile of v8, /device:TPU:224, one launch (start us, length us, event | category | flops | bytes accessed | tf_op | source)
XLA Modules:
  0.0 60.8 jit_solution(11299267966703389427)
XLA Ops:
  0.0 59.2 %shard_map.91 = bf16[64,1024]{1,0:T(8,128)(2,1)} custom-call(bf16[64,1024]{1,0:T(8,128)(2,1)} %tokens_ref.1, f32[1,1024]{1,0:T(1,128)} %bitcast.3, bf16[16,256]{1,0:T(8,128)(2,1)} %wq_ref.1, bf16[16,256]{1,0:T(8,128)(2,1)} %wk_ref.1, bf16[16,256]{1,0:T(8,128)(2,1)} %wv_ref.1, bf16[4,16]{1,0:T(4,128)(2,1)} %bitcast.5, f32[4]{0:T(128)} %offset_ref.1, ...), custom_call_target="tpu_custom_call" | custom-call | tf_op jit(solution)/shard_map/pallas_call | solution.py:666
  59.2 1.6 %copy.11 = bf16[64,1024]{1,0:T(8,128)(2,1)} copy(bf16[64,1024]{1,0:T(8,128)(2,1)} %shard_map.91) | data formatting | bytes 262144

commit v9 on v8

--- a/solution.py
+++ b/solution.py
@@ -184,7 +184,9 @@
 
     def twin(ref, send, recv, way, step, sub):
         place = ref.at[plane_at(way, step), wrap(x + sub, NX), c]
-        return remote(place, place, send.at[way, step], recv.at[way, step], z, x, other, tp)
+        return remote(
+            place, place, send.at[way, step], recv.at[way, step, sub // 2], z, x, other, tp
+        )
 
     def tok_copy(dy):
         return remote(
@@ -444,13 +446,15 @@
     lane_block = lax.broadcasted_iota(jnp.int32, (8, LANES), 1) % 8
     ones_rows = jnp.ones((16, CHUNK * half), BF16)
 
-    def attend(plane, own, core=None):
-        if core is None:
+    def attend(plane, own, duo=None):
+        if duo is None:
             blocks = [(b // NC, b % NC) for b in range(plane_blocks)]
             key_rows = kv_all[plane, :, :, :half, :].reshape(plane_blocks * half, LANES)
         else:
-            blocks = [(b, core) for b in range(NX)]
-            key_rows = kv_all[plane, :, core, :half, :].reshape(NX * half, LANES)
+            blocks = [(wrap(x + 2 * duo + d, NX), cc) for d in (0, 1) for cc in range(NC)]
+            key_rows = jnp.concatenate(
+                [kv_all[plane, xx, cc, :half, :] for xx, cc in blocks], axis=0
+            )
         bias_cols = bias_all[plane]
         masks = [
             jnp.where(lane_block == xx * NC + cc, 1.0, 0.0)[:1].astype(BF16)
@@ -505,7 +509,8 @@
             if n >= LAG:
                 absorb(*chunks[n - LAG], tops[n - LAG])
 
-    landed(kv_all.at[z, :, other], kd_recv.at[0, 0])
+    for pair in (0, 1):
+        landed(kv_all.at[z, pl.ds(0, NX // 2), other], kd_recv.at[0, 0, pair])
     attend(z, True)
     first_sub(2)
 
@@ -520,44 +525,47 @@
             for way in both:
                 ring_poll(way, step, sub)
 
-    def twin_step(step):
-        for way in both:
-
-            @pl.when(reads(way, step) & (step < far))
-            def _():
-                landed(kv_all.at[plane_at(way, step), :, other], kd_recv.at[way, step])
-
-            @pl.when(reads(way, step) & (step == far))
-            def _():
-                landed(
-                    kv_all.at[plane_at(way, step), pl.ds(0, NX // 2), other],
-                    kd_recv.at[way, step],
-                )
-
-    def maybe_attend(plane, extra, core=None):
-        @pl.when((plane < z) & extra)
+    def twin_wait(plane, way, step, duo):
+        landed(kv_all.at[plane, pl.ds(0, NX // 2), other], kd_recv.at[way, step, duo])
+
+    kv_step(1, (1,))
+
+    @pl.loop(0, 2)
+    def _(way):
+        plane = jnp.where(way == 0, wrap(z - 1, nz), wrap(z + 1, nz))
+
+        @pl.when(plane < z)
         def _():
-            attend(plane, False, core)
-
-    kv_step(1, (1,))
+            twin_wait(plane, way, 1, 0)
+            attend(plane, False, 0)
 
     @pl.loop(1, far + 1)
     def _(step):
         kv_step(step, (2,))
+        pl.when(step == 2)(lambda: kv_step(2, (1,)))
         pl.when(step == 2)(lambda: first_sub(3))
         pl.when(step == 3)(lambda: first_sub(4))
-        maybe_attend(plane_at(1, step - 1), step > 1)
+        @pl.when((step > 2) & reads(1, step - 1))
+        def _():
+            plane = plane_at(1, step - 1)
+            for duo in (0, 1):
+                twin_wait(plane, 1, step - 1, duo)
+            attend(plane, False)
+
         kv_step(step, (3,))
         pl.when(step == 1)(wo_along_y)
 
-        @pl.loop(0, NC)
+        @pl.loop(jnp.where(step == 1, 1, 0), jnp.where(step == 1, 3, 2))
         def _(part):
-            @pl.when(part == 1)
+            pl.when((part == 1) & (step > 1))(lambda: kv_step(step + 1, (1,)))
+            duo = jnp.minimum(part, 1)
+            plane = jnp.where(part == 2, wrap(z + 1, nz), wrap(z - step, nz))
+
+            @pl.when(plane < z)
             def _():
-                twin_step(step)
-                kv_step(step + 1, (1,))
-
-            maybe_attend(plane_at(0, step), True, lax.rem(c + part, NC))
+                way = jnp.where(step == far, duo, jnp.where(part == 2, 1, 0))
+                twin_wait(plane, way, step, duo)
+                attend(plane, False, duo)
 
 
     my_head = tp * NX + x
@@ -708,7 +716,7 @@
                 dma((1,)), dma((NX - 1,)),
                 *pair(1),
                 *pair(2, far, NX),
-                *pair(2, far + 1),
+                dma((2, far + 1)), dma((2, far + 1, 2)),
                 *pair(1),
             ],
             compiler_params=pltpu.CompilerParams(collective_id=0, has_side_effects=True),

time: 61.3 us -> 62.5 us (1.020)
  Pallas kernels: 59.2 us -> 60.5 us
    pallas_call x1, Pallas kernels: 59.2 us -> 60.5 us  [on_device(): pl.pallas_call(functools.partial(layer_kernel, nz, n_tp), out_shape=jax.S...]
where the time goes in v9:
time: 62.5 us; the launch traced here: 62 us
  Pallas kernels  60.5 us (97%)
  local copies, waits for them, and re-layouts  1.57 us (3%)
    pallas_call x1, Pallas kernels, on_device(): pl.pallas_call(functools.partial(layer_kernel, nz, n_tp), out_shape=jax.S...  60.5 us
    unnamed x1, local copies, waits for them, and re-layouts  1.57 us

profile of v9, /device:TPU:224, one launch (start us, length us, event | category | flops | bytes accessed | tf_op | source)
XLA Modules:
  0.0 62.0 jit_solution(4068126753020949956)
XLA Ops:
  0.0 60.5 %shard_map.91 = bf16[64,1024]{1,0:T(8,128)(2,1)} custom-call(bf16[64,1024]{1,0:T(8,128)(2,1)} %tokens_ref.1, f32[1,1024]{1,0:T(1,128)} %bitcast.3, bf16[16,256]{1,0:T(8,128)(2,1)} %wq_ref.1, bf16[16,256]{1,0:T(8,128)(2,1)} %wk_ref.1, bf16[16,256]{1,0:T(8,128)(2,1)} %wv_ref.1, bf16[4,16]{1,0:T(4,128)(2,1)} %bitcast.5, f32[4]{0:T(128)} %offset_ref.1, ...), custom_call_target="tpu_custom_call" | custom-call | tf_op jit(solution)/shard_map/pallas_call | solution.py:674
  60.5 1.6 %copy.11 = bf16[64,1024]{1,0:T(8,128)(2,1)} copy(bf16[64,1024]{1,0:T(8,128)(2,1)} %shard_map.91) | data formatting | bytes 262144

commit v10 on v7

--- a/solution.py
+++ b/solution.py
@@ -111,7 +111,7 @@
     def w_x(a, k, dx):
         place = w_place(a, k, 0, c)
         return remote(
-            place, place, wx_send.at[a], wx_recv.at[a, k],
+            place, place, wx_send.at[a], wx_recv.at[a * nz + k],
             z, wrap(x + dx, NX), c, tp,
         )
 
@@ -143,7 +143,7 @@
         @pl.loop(first, last)
         def _(n):
             k = jnp.where(n == 0, 0, nearest(n))
-            landed(w_kv.at[0, pl.ds(0, NX - 1), c], wx_recv.at[0, k])
+            landed(w_kv.at[0, pl.ds(0, NX - 1), c], wx_recv.at[k])
             w_twin(0, k).start()
 
     def w_from_twin(a):
@@ -173,7 +173,7 @@
     def ring_hop(ref, send, recv, way, step, sub):
         place = ref.at[plane_at(way, step - 1), wrap(x + sub, NX), c]
         return remote(
-            place, place, send.at[way, step - 1, sub], recv.at[way, step - 1, sub],
+            place, place, send.at[way, step - 1, sub // 2], recv.at[way, step - 1, sub],
             (up, down)[way], x, c, tp,
         )
 
@@ -243,7 +243,7 @@
 
     w_onward(0, 0)
     w_from_z(0, 1, 3)
-    landed(w_q.at[0, pl.ds(0, NX - 1), c], wx_recv.at[1, 0])
+    landed(w_q.at[0, pl.ds(0, NX - 1), c], wx_recv.at[nz])
     for k in far_first:
         w_group_z(k).start()
     for k in far_first:
@@ -543,10 +543,10 @@
     def _(step):
         kv_step(step, (1,))
         pl.when(step == 2)(lambda: first_sub(3))
-        pl.when(step == 2)(wo_along_y)
         pl.when(step == 3)(lambda: first_sub(4))
         maybe_attend(plane_at(1, step - 1), step > 1)
         kv_step(step, (2, 3))
+        pl.when(step == 1)(wo_along_y)
 
         @pl.loop(0, NC)
         def _(part):
@@ -628,12 +628,12 @@
             def _():
                 left(kv_all.at[0, pl.ds(0, count), 0], kd_send.at[way, step])
 
-            for sub in range(NX):
-                if step <= steps_of(way, sub):
-
-                    @pl.when(sends(way, step, sub))
+            for duo in (0, 1):
+                if step <= steps_of(way, 2 * duo):
+
+                    @pl.when(sends(way, step, 2 * duo))
                     def _():
-                        left(kv_all.at[0, 0, 0], kz_send.at[way, step - 1, sub])
+                        left(kv_all.at[0, pl.ds(0, 2), 0], kz_send.at[way, step - 1, duo])
     left(att_recv.at[pl.ds(0, NX * n_tp - 1)], at_send.at[0])
 
 
@@ -688,7 +688,7 @@
                 dma((4,)),
                 *pair(1),
                 dma((2,)), dma((2, nz)),
-                dma((2,)), dma((2, nz)),
+                dma((2,)), dma((nz + 1,)),
                 *pair(2),
                 *pair(1),
                 *pair(1),
@@ -701,7 +701,7 @@
                 *pair(2),
                 dma((1,)), dma((NX - 1,)),
                 *pair(1),
-                *pair(2, far, NX),
+                dma((2, far, 2)), dma((2, far, NX)),
                 *pair(2, far + 1),
                 *pair(1),
             ],

time: 60.4 us -> 60.2 us (level)
  no operation moved by 1% of the time
where the time goes in v10:
time: 60.2 us; the launch traced here: 59.8 us
  Pallas kernels  58.2 us (97%)
  local copies, waits for them, and re-layouts  1.57 us (3%)
    pallas_call x1, Pallas kernels, on_device(): pl.pallas_call(functools.partial(layer_kernel, nz, n_tp), out_shape=jax.S...  58.2 us
    unnamed x1, local copies, waits for them, and re-layouts  1.57 us

profile of v10, /device:TPU:224, one launch (start us, length us, event | category | flops | bytes accessed | tf_op | source)
XLA Modules:
  0.0 59.8 jit_solution(6215274663583947542)
XLA Ops:
  0.0 58.2 %shard_map.91 = bf16[64,1024]{1,0:T(8,128)(2,1)} custom-call(bf16[64,1024]{1,0:T(8,128)(2,1)} %tokens_ref.1, f32[1,1024]{1,0:T(1,128)} %bitcast.3, bf16[16,256]{1,0:T(8,128)(2,1)} %wq_ref.1, bf16[16,256]{1,0:T(8,128)(2,1)} %wk_ref.1, bf16[16,256]{1,0:T(8,128)(2,1)} %wv_ref.1, bf16[4,16]{1,0:T(4,128)(2,1)} %bitcast.5, f32[4]{0:T(128)} %offset_ref.1, ...), custom_call_target="tpu_custom_call" | custom-call | tf_op jit(solution)/shard_map/pallas_call | solution.py:660
  58.2 1.6 %copy.11 = bf16[64,1024]{1,0:T(8,128)(2,1)} copy(bf16[64,1024]{1,0:T(8,128)(2,1)} %shard_map.91) | data formatting | bytes 262144

commit v11 on v10

--- a/solution.py
+++ b/solution.py
@@ -541,11 +541,11 @@
 
     @pl.loop(1, far + 1)
     def _(step):
-        kv_step(step, (1,))
+        kv_step(step, (1, 2))
         pl.when(step == 2)(lambda: first_sub(3))
         pl.when(step == 3)(lambda: first_sub(4))
         maybe_attend(plane_at(1, step - 1), step > 1)
-        kv_step(step, (2, 3))
+        kv_step(step, (3,))
         pl.when(step == 1)(wo_along_y)
 
         @pl.loop(0, NC)

time: 60.2 us -> 61 us (1.013)
  Pallas kernels: 58.2 us -> 59 us
    pallas_call x1, Pallas kernels: 58.2 us -> 59 us  [on_device(): pl.pallas_call(functools.partial(layer_kernel, nz, n_tp), out_shape=jax.S...]
where the time goes in v11:
time: 61 us; the launch traced here: 60.6 us
  Pallas kernels  59 us (97%)
  local copies, waits for them, and re-layouts  1.57 us (3%)
    pallas_call x1, Pallas kernels, on_device(): pl.pallas_call(functools.partial(layer_kernel, nz, n_tp), out_shape=jax.S...  59 us
    unnamed x1, local copies, waits for them, and re-layouts  1.57 us

profile of v11, /device:TPU:224, one launch (start us, length us, event | category | flops | bytes accessed | tf_op | source)
XLA Modules:
  0.0 60.6 jit_solution(12478001184507012045)
XLA Ops:
  0.0 59.0 %shard_map.91 = bf16[64,1024]{1,0:T(8,128)(2,1)} custom-call(bf16[64,1024]{1,0:T(8,128)(2,1)} %tokens_ref.1, f32[1,1024]{1,0:T(1,128)} %bitcast.3, bf16[16,256]{1,0:T(8,128)(2,1)} %wq_ref.1, bf16[16,256]{1,0:T(8,128)(2,1)} %wk_ref.1, bf16[16,256]{1,0:T(8,128)(2,1)} %wv_ref.1, bf16[4,16]{1,0:T(4,128)(2,1)} %bitcast.5, f32[4]{0:T(128)} %offset_ref.1, ...), custom_call_target="tpu_custom_call" | custom-call | tf_op jit(solution)/shard_map/pallas_call | solution.py:660
  59.0 1.6 %copy.11 = bf16[64,1024]{1,0:T(8,128)(2,1)} copy(bf16[64,1024]{1,0:T(8,128)(2,1)} %shard_map.91) | data formatting | bytes 262144

commit v12 on v10

--- a/solution.py
+++ b/solution.py
@@ -545,7 +545,7 @@
         pl.when(step == 2)(lambda: first_sub(3))
         pl.when(step == 3)(lambda: first_sub(4))
         maybe_attend(plane_at(1, step - 1), step > 1)
-        kv_step(step, (2, 3))
+        kv_step(step, (3, 2))
         pl.when(step == 1)(wo_along_y)
 
         @pl.loop(0, NC)

time: 60.2 us -> 60.2 us (level)
  no operation moved by 1% of the time
where the time goes in v12:
time: 60.2 us; the launch traced here: 59.8 us
  Pallas kernels  58.2 us (97%)
  local copies, waits for them, and re-layouts  1.57 us (3%)
    pallas_call x1, Pallas kernels, on_device(): pl.pallas_call(functools.partial(layer_kernel, nz, n_tp), out_shape=jax.S...  58.2 us
    unnamed x1, local copies, waits for them, and re-layouts  1.57 us

profile of v12, /device:TPU:224, one launch (start us, length us, event | category | flops | bytes accessed | tf_op | source)
XLA Modules:
  0.0 59.8 jit_solution(12244210502824002824)
XLA Ops:
  0.0 58.2 %shard_map.91 = bf16[64,1024]{1,0:T(8,128)(2,1)} custom-call(bf16[64,1024]{1,0:T(8,128)(2,1)} %tokens_ref.1, f32[1,1024]{1,0:T(1,128)} %bitcast.3, bf16[16,256]{1,0:T(8,128)(2,1)} %wq_ref.1, bf16[16,256]{1,0:T(8,128)(2,1)} %wk_ref.1, bf16[16,256]{1,0:T(8,128)(2,1)} %wv_ref.1, bf16[4,16]{1,0:T(4,128)(2,1)} %bitcast.5, f32[4]{0:T(128)} %offset_ref.1, ...), custom_call_target="tpu_custom_call" | custom-call | tf_op jit(solution)/shard_map/pallas_call | solution.py:660
  58.2 1.6 %copy.11 = bf16[64,1024]{1,0:T(8,128)(2,1)} copy(bf16[64,1024]{1,0:T(8,128)(2,1)} %shard_map.91) | data formatting | bytes 262144
